TPU v7x, 256 devices: a whole 4x4x8 slice. The times are simulated.
256 devices in a mesh: kv: 32 (over z, x), tp: 8 (over y, core).
Axes of the slice: x: 4, y: 4, z: 8, core: 2. Of those that a mesh axis runs over, the one named last changes fastest.
Arguments:
- tokens: bfloat16 [1024, 2048], P('kv', 'tp'), may hold values from -60 to 60, as said below
- memory: float32 [1024, 8, 128, 128], P('kv', 'tp'), may hold values from -0.6 to 0.6
- normalizer: float32 [1024, 8, 128], P('kv', 'tp'), may hold values from -0.6 to 0.6
- stabilizer: float32 [1024, 8], P('kv', 'tp'), may hold values from -4 to 4
- norm_gain: float32 [2048], replicated, may hold values from 0.1 to 1.9
- query_weight: bfloat16 [2048, 1024], P(None, 'tp'), may hold values from -0.125 to 0.125
- key_weight: bfloat16 [2048, 1024], P(None, 'tp'), may hold values from -0.125 to 0.125
- value_weight: bfloat16 [2048, 1024], P(None, 'tp'), may hold values from -0.125 to 0.125
- outgate_weight: bfloat16 [2048, 1024], P(None, 'tp'), may hold values from -0.125 to 0.125
- input_gate_weight: bfloat16 [2048, 8], replicated, may hold values from -0.125 to 0.125
- forget_gate_weight: bfloat16 [2048, 8], replicated, may hold values from -0.125 to 0.125
- forget_bias: float32 [8], replicated, may hold values from -1 to 5
- memory_gain: float32 [1024], P('tp'), may hold values from 0.1 to 1.9
- proj_weight: bfloat16 [1024, 2048], P(None, 'tp'), may hold values from -0.1875 to 0.1875
- ffn_gain: float32 [2048], P('tp'), may hold values from 0.1 to 1.9
- up_weight: bfloat16 [2048, 8192], P('tp', 'kv'), may hold values from -0.125 to 0.125
- down_weight: bfloat16 [8192, 2048], P('kv', 'tp'), may hold values from -0.0625 to 0.0625
Outputs:
- layer_out: bfloat16 [1024, 2048], P('kv', 'tp')
- memory_new: float32 [1024, 8, 128, 128], P('kv', 'tp')
- normalizer_new: float32 [1024, 8, 128], P('kv', 'tp')
- stabilizer_new: float32 [1024, 8], P('kv', 'tp')
Inputs may be any that keep to these rules, and one draw needn't show every extreme that they name: `tokens`: activations whose feature blocks and rows differ in scale.
All inputs are finite; a program needn't handle non-finite values.
Results may differ from a plain program's by a relative error of at most 0.0095.
Values may be sent and summed in bfloat16 or wider, within the bound.
A program may use at most 64 MiB of HBM per device.

v0:
```python
import jax
import jax.numpy as jnp
from jax import lax
from jax.sharding import PartitionSpec as P

D = 2048
DK = 128
DV = 128


EPS = 1e-06


def from_everyone(value, axis):
    copies = jnp.broadcast_to(value, (lax.axis_size(axis), *value.shape))
    return lax.all_to_all(copies, axis, split_axis=0, concat_axis=0, tiled=True)


def laid_out(blocks, dim):
    blocks = jnp.moveaxis(blocks, 0, dim)
    shape = blocks.shape
    return blocks.reshape(*shape[:dim], shape[dim] * shape[dim + 1], *shape[dim + 2 :])


def gathered_copies(value, axis, dim):
    blocks = from_everyone(value, axis)
    return laid_out(blocks, dim)


def cut_along(value, dim, peers):
    shape = value.shape
    blocks = value.reshape(*shape[:dim], peers, shape[dim] // peers, *shape[dim + 1 :])
    return jnp.moveaxis(blocks, dim, 0)


def sum_at_owner(value, axis, dim):
    blocks = cut_along(value, dim, lax.axis_size(axis))
    arrived = lax.all_to_all(blocks, axis, split_axis=0, concat_axis=0, tiled=True)
    return arrived.astype(jnp.float32).sum(axis=0)


def of_everyone(value, axis):
    everything = from_everyone(value, axis)
    return jnp.sum(everything, axis=0)


def per_device(
    tokens,
    memory,
    normalizer,
    stabilizer,
    norm_gain,
    query_weight,
    key_weight,
    value_weight,
    outgate_weight,
    input_gate_weight,
    forget_gate_weight,
    forget_bias,
    memory_gain,
    proj_weight,
    ffn_gain,
    up_weight,
    down_weight,
):
    own_rows = tokens.shape[0]
    heads_here = memory.shape[1]
    first_head = lax.axis_index("tp") * heads_here
    full_rows = gathered_copies(tokens, "tp", 1)
    rows_f = full_rows.astype(jnp.float32)
    scale_one = lax.rsqrt(jnp.mean(rows_f * rows_f, axis=-1, keepdims=True) + EPS)
    normed = (rows_f * scale_one * norm_gain).astype(jnp.bfloat16)
    query = jnp.dot(normed, query_weight, preferred_element_type=jnp.float32).astype(jnp.bfloat16)
    keys = jnp.dot(normed, key_weight, preferred_element_type=jnp.float32).astype(jnp.bfloat16)
    values = jnp.dot(normed, value_weight, preferred_element_type=jnp.float32).astype(jnp.bfloat16)
    gate_out = jnp.dot(normed, outgate_weight, preferred_element_type=jnp.float32).astype(
        jnp.bfloat16
    )
    input_cols = lax.dynamic_slice_in_dim(input_gate_weight, first_head, heads_here, 1)
    forget_cols = lax.dynamic_slice_in_dim(forget_gate_weight, first_head, heads_here, 1)
    bias_here = lax.dynamic_slice_in_dim(forget_bias, first_head, heads_here, 0)
    input_log = jnp.dot(normed, input_cols, preferred_element_type=jnp.float32)
    forget_log = jax.nn.log_sigmoid(
        jnp.dot(normed, forget_cols, preferred_element_type=jnp.float32) + bias_here
    )
    query_f = query.astype(jnp.float32).reshape(own_rows, heads_here, DK)
    keys_f = keys.astype(jnp.float32).reshape(own_rows, heads_here, DK) * DK ** (-0.5)
    values_f = values.astype(jnp.float32).reshape(own_rows, heads_here, DV)
    stab_new = jnp.maximum(forget_log + stabilizer, input_log)
    keep = jnp.exp(forget_log + stabilizer - stab_new)
    admit = jnp.exp(input_log - stab_new)
    memory_new = (
        keep[..., None, None] * memory
        + admit[..., None, None] * values_f[..., :, None] * keys_f[..., None, :]
    )
    normalizer_new = keep[..., None] * normalizer + admit[..., None] * keys_f
    numer = jnp.einsum("bhed,bhd->bhe", memory_new, query_f, precision=lax.Precision.HIGHEST)
    denom = jnp.sum(normalizer_new * query_f, axis=-1)
    cell = numer / jnp.maximum(jnp.abs(denom), 1.0)[..., None]
    mixed = (
        cell.reshape(own_rows, heads_here * DV)
        * memory_gain
        * jax.nn.sigmoid(gate_out.astype(jnp.float32))
    ).astype(jnp.bfloat16)
    projected = jnp.dot(
        gathered_copies(mixed, "tp", 1), proj_weight, preferred_element_type=jnp.float32
    )
    second = (tokens.astype(jnp.float32) + projected).astype(jnp.bfloat16)
    all_rows = gathered_copies(second, "kv", 0)
    all_f = all_rows.astype(jnp.float32)
    square_sum = jnp.sum(all_f * all_f, axis=-1)
    scaled = (all_f * ffn_gain).astype(jnp.bfloat16)
    preact = jnp.dot(scaled, up_weight, preferred_element_type=jnp.float32)
    share = sum_at_owner(preact.astype(jnp.bfloat16), "tp", 1)
    square_sum = of_everyone(square_sum, "tp")
    scale_two = lax.rsqrt(square_sum / D + EPS)
    partial_hidden = jnp.square(jax.nn.relu(share * scale_two[:, None])).astype(jnp.bfloat16)
    hidden = gathered_copies(partial_hidden, "tp", 1)
    summed = sum_at_owner(
        jnp.dot(hidden, down_weight, preferred_element_type=jnp.float32).astype(jnp.bfloat16),
        "kv",
        0,
    )
    layer_out = (second.astype(jnp.float32) + summed).astype(jnp.bfloat16)
    return (layer_out, memory_new, normalizer_new, stab_new)


def solution(mesh):
    placed = (
        P("kv", "tp"),
        P("kv", "tp", None, None),
        P("kv", "tp", None),
        P("kv", "tp"),
        P(),
        P(None, "tp"),
        P(None, "tp"),
        P(None, "tp"),
        P(None, "tp"),
        P(),
        P(),
        P(),
        P("tp"),
        P(None, "tp"),
        P("tp"),
        P("tp", "kv"),
        P("kv", "tp"),
    )
    return jax.shard_map(
        per_device,
        mesh=mesh,
        in_specs=placed,
        out_specs=(P("kv", "tp"), P("kv", "tp", None, None), P("kv", "tp", None), P("kv", "tp")),
        check_vma=False,
    )
```

profile of v0, /device:TPU:1, one launch (start us, length us, event | category | flops | bytes accessed | tf_op | source)
XLA Modules:
  0.0 114.5 jit_solution(16358891694366830972)
XLA Ops:
  0.6 0.0 copy-start
  0.6 0.0 copy-start.10
  0.7 0.0 copy-start.4
  0.7 0.0 copy-start.11
  0.7 0.0 copy-start.5
  0.7 1.5 %broadcast_in_dim.12 = bf16[8,32,256]{2,1,0:T(8,128)(2,1)} broadcast(bf16[32,256]{1,0:T(8,128)(2,1)} %param.17), dimensions={1,2} | broadcast | bytes 147456 | tf_op jit(solution)/shard_map/broadcast_in_dim | solution.py:15
  2.2 6.5 %all-to-all-start = ((bf16[8,32,256]{2,1,0:T(8,128)(2,1)}), bf16[8,32,256]{2,1,0:T(8,128)(2,1)S(1)}, u32[]{:S(2)}, u32[]{:S(2)}) async-start(bf16[8,32,256]{2,1,0:T(8,128)(2,1)} %broadcast_in_dim.12), calls=%async_computation | async-start | bytes 262144 | tf_op jit(solution)/shard_map/all_to_all | solution.py:16
  8.7 0.7 mul.148
  9.4 1.2 %dynamic_slice.10 = f32[1]{0:T(128)} dynamic-slice(f32[8]{0:T(128)} %param.28, s32[]{:T(128)S(6)} %select_n.11), dynamic_slice_sizes={1} | dynamic-slice | bytes 12 | tf_op jit(solution)/shard_map/dynamic_slice | solution.py:81
  10.6 3.3 %all-to-all-done = bf16[8,32,256]{2,1,0:T(8,128)(2,1)S(1)} async-done(((bf16[8,32,256]{2,1,0:T(8,128)(2,1)}), bf16[8,32,256]{2,1,0:T(8,128)(2,1)S(1)}, u32[]{:S(2)}, u32[]{:S(2)}) %all-to-all-start) | async-done | bytes 131104 | tf_op jit(solution)/shard_map/all_to_all | solution.py:16
  13.9 0.1 fusion.16
  14.1 0.0 copy-start.2
  14.1 0.1 fusion.19
  14.2 1.7 %bitcast_add_fusion.1 = f32[32,1]{0,1:T(1,128)S(1)} fusion(f32[32,1]{0,1:T(1,128)} %param.20, bf16[32,2048]{1,0:T(8,128)(2,1)S(1)} %bitcast.79, bf16[2048,8]{0,1:T(8,128)(2,1)} %param.27, s32[]{:T(128)S(6)} %select_n.11, f32[]{:T(128)} %bitcast.2), kind=kOutput, calls=%fused_computation.52 | convolution fusion | flops 131392 | bytes 140420 | tf_op jit(solution)/shard_map/dot_general | solution.py:84
  15.9 0.9 broadcast_multiply_fusion.1
  16.9 0.0 copy-done.10
  16.9 0.1 multiply_convert_fusion
  17.0 0.0 copy-done.4
  17.0 0.2 broadcast_multiply_fusion
  17.2 0.0 copy-done
  17.2 0.0 copy-done.11
  17.2 0.9 fusion.22
  18.1 0.0 copy-done.5
  18.1 0.2 fusion.12
  18.4 0.0 copy-done.2
  18.4 0.8 multiply_add_fusion
  19.1 0.0 copy-done.13
  19.1 0.0 copy-start.1
  19.2 0.0 copy-start.6
  19.2 0.0 copy-start.14
  19.2 0.0 copy-start.3
  19.2 0.0 copy-start.9
  19.2 1.7 %fusion = f32[32,1,128]{2,1,0:T(1,128)S(1)} fusion(f32[32,1,128,128]{3,2,1,0:T(8,128)S(1)} %multiply_add_fusion, bf16[32,128,1]{1,0,2:T(8,128)(2,1)S(1)} %bitcast.82), kind=kOutput, calls=%fused_computation | convolution fusion | flops 6291456 | bytes 2121728 | tf_op jit(solution)/shard_map/bhed,bhd->bhe/dot_general | solution.py:97
  20.9 0.0 copy-done.6
  20.9 0.0 copy-done.14
  21.0 0.2 fusion.9
  21.2 0.0 copy-start.7
  21.2 8.2 %all_to_all.36 = bf16[8,32,128]{2,1,0:T(8,128)(2,1)S(1)} all-to-all(bf16[8,32,128]{2,1,0:T(8,128)(2,1)S(1)} %broadcast_in_dim.13), channel_id=1, replica_groups=mesh['kv'=32,'tp'=8] {'tp'}, dimensions={0} | all-to-all | bytes 131072 | tf_op jit(solution)/shard_map/all_to_all | solution.py:16
  29.4 0.0 copy-done.3
  29.4 0.0 copy-done.9
  29.4 0.2 fusion.2
  29.6 0.1 broadcast_in_dim.14
  29.7 26.3 %all_to_all.37 = bf16[32,32,256]{2,1,0:T(8,128)(2,1)S(1)} all-to-all(bf16[32,32,256]{2,1,0:T(8,128)(2,1)S(1)} %broadcast_in_dim.14), channel_id=1, replica_groups=mesh['kv'=32,'tp'=8] {'kv'}, dimensions={0} | all-to-all | bytes 1048576 | tf_op jit(solution)/shard_map/all_to_all | solution.py:16
  56.0 0.0 copy-done.1
  56.0 0.2 multiply_reduce_fusion
  56.2 0.1 broadcast_in_dim.15
  56.3 0.6 broadcast_in_dim.16
  57.0 5.8 %all-to-all-start.4 = ((f32[8,1,1024]{2,1,0:T(1,128)}), f32[8,1,1024]{2,1,0:T(1,128)S(1)}, u32[]{:S(2)}, u32[]{:S(2)}) async-start(f32[8,1,1024]{2,1,0:T(1,128)} %broadcast_in_dim.16), calls=%async_computation.4 | async-start | bytes 65536 | tf_op jit(solution)/shard_map/all_to_all | solution.py:16
  62.8 0.0 copy-done.12
  62.8 0.1 fusion.15
  62.9 0.0 copy-done.7
  62.9 0.0 copy-start.8
  62.9 1.1 convolution_convert_fusion.1
  64.1 3.5 %all-to-all-done.4 = f32[8,1,1024]{2,1,0:T(1,128)S(1)} async-done(((f32[8,1,1024]{2,1,0:T(1,128)}), f32[8,1,1024]{2,1,0:T(1,128)S(1)}, u32[]{:S(2)}, u32[]{:S(2)}) %all-to-all-start.4) | async-done | bytes 32800 | tf_op jit(solution)/shard_map/all_to_all | solution.py:16
  67.5 4.1 %all-to-all-start.3 = ((bf16[8,1024,32]{1,2,0:T(8,128)(2,1)}), bf16[8,1024,32]{1,2,0:T(8,128)(2,1)S(1)}, u32[]{:S(2)}, u32[]{:S(2)}) async-start(bf16[8,1024,32]{1,2,0:T(8,128)(2,1)} %bitcast.19), calls=%async_computation.3 | async-start | bytes 1048576 | tf_op jit(solution)/shard_map/all_to_all | solution.py:38
  71.7 9.3 %all-to-all-done.3 = bf16[8,1024,32]{1,2,0:T(8,128)(2,1)S(1)} async-done(((bf16[8,1024,32]{1,2,0:T(8,128)(2,1)}), bf16[8,1024,32]{1,2,0:T(8,128)(2,1)S(1)}, u32[]{:S(2)}, u32[]{:S(2)}) %all-to-all-start.3) | async-done | bytes 524320 | tf_op jit(solution)/shard_map/all_to_all | solution.py:38
  81.0 0.1 convert_reduce_fusion.1
  81.2 0.1 broadcast_in_dim.34
  81.2 12.7 %all_to_all.38 = bf16[8,1024,32]{1,2,0:T(8,128)(2,1)S(1)} all-to-all(bf16[8,1024,32]{1,2,0:T(8,128)(2,1)S(1)} %broadcast_in_dim.34), channel_id=1, replica_groups=mesh['kv'=32,'tp'=8] {'tp'}, dimensions={0} | all-to-all | bytes 1048576 | tf_op jit(solution)/shard_map/all_to_all | solution.py:16
  93.9 0.0 copy-done.8
  93.9 0.4 convolution_convert_fusion
  94.3 19.6 %all_to_all.39 = bf16[32,32,256]{2,1,0:T(8,128)(2,1)S(1)} all-to-all(bf16[32,32,256]{2,1,0:T(8,128)(2,1)S(1)} %bitcast.78), channel_id=1, replica_groups=mesh['kv'=32,'tp'=8] {'kv'}, dimensions={0} | all-to-all | bytes 1048576 | tf_op jit(solution)/shard_map/all_to_all | solution.py:38
  113.8 0.1 convert_reduce_fusion
  113.9 0.6 add_convert_fusion
  (12 shorter events, 0.2 us)
Async XLA Ops:
  0.6 16.6 %copy-start = (bf16[2048,128]{1,0:T(8,128)(2,1)S(1)}, bf16[2048,128]{1,0:T(8,128)(2,1)}, u32[]{:S(2)}) copy-start(bf16[2048,128]{1,0:T(8,128)(2,1)} %param.22) | copy-start | bytes 1572868
  0.6 16.3 %copy-start.10 = (f32[2048]{0:T(1024)S(1)}, f32[2048]{0:T(1024)}, u32[]{:S(2)}) copy-start(f32[2048]{0:T(1024)} %param.21) | copy-start | bytes 24580
  0.7 16.3 %copy-start.4 = (bf16[2048,128]{1,0:T(8,128)(2,1)S(1)}, bf16[2048,128]{1,0:T(8,128)(2,1)}, u32[]{:S(2)}) copy-start(bf16[2048,128]{1,0:T(8,128)(2,1)} %param.23) | copy-start | bytes 1572868
  0.7 16.6 %copy-start.11 = (f32[32,1,128]{2,1,0:T(1,128)S(1)}, f32[32,1,128]{2,1,0:T(1,128)}, u32[]{:S(2)}) copy-start(f32[32,1,128]{2,1,0:T(1,128)} %param.19) | copy-start | bytes 49156
  0.7 17.5 %copy-start.5 = (bf16[2048,128]{1,0:T(8,128)(2,1)S(1)}, bf16[2048,128]{1,0:T(8,128)(2,1)}, u32[]{:S(2)}) copy-start(bf16[2048,128]{1,0:T(8,128)(2,1)} %param.24) | copy-start | bytes 1572868
  2.2 11.7 %all-to-all-start = ((bf16[8,32,256]{2,1,0:T(8,128)(2,1)}), bf16[8,32,256]{2,1,0:T(8,128)(2,1)S(1)}, u32[]{:S(2)}, u32[]{:S(2)}) async-start(bf16[8,32,256]{2,1,0:T(8,128)(2,1)} %broadcast_in_dim.12), calls=%async_computation | async-start | bytes 262144 | tf_op jit(solution)/shard_map/all_to_all | solution.py:16
  14.1 4.3 %copy-start.2 = (f32[32,1,128,128]{3,2,1,0:T(8,128)S(1)}, f32[32,1,128,128]{3,2,1,0:T(8,128)}, u32[]{:S(2)}) copy-start(f32[32,1,128,128]{3,2,1,0:T(8,128)} %param.18) | copy-start | bytes 6291460
  16.8 2.3 %copy-start.13 = (f32[32,1]{0,1:T(1,128)}, f32[32,1]{0,1:T(1,128)S(1)}, u32[]{:S(2)}) copy-start(f32[32,1]{0,1:T(1,128)S(1)} %get-tuple-element.28) | copy-start | bytes 388
  19.1 36.9 %copy-start.1 = (f32[32,1,128,128]{3,2,1,0:T(8,128)}, f32[32,1,128,128]{3,2,1,0:T(8,128)S(1)}, u32[]{:S(2)}) copy-start(f32[32,1,128,128]{3,2,1,0:T(8,128)S(1)} %multiply_add_fusion) | copy-start | bytes 6291460
  19.2 1.8 %copy-start.6 = (bf16[2048,128]{1,0:T(8,128)(2,1)S(1)}, bf16[2048,128]{1,0:T(8,128)(2,1)}, u32[]{:S(2)}) copy-start(bf16[2048,128]{1,0:T(8,128)(2,1)} %param.25) | copy-start | bytes 1572868
  19.2 1.8 %copy-start.14 = (f32[128]{0:T(128)S(1)}, f32[128]{0:T(128)}, u32[]{:S(2)}) copy-start(f32[128]{0:T(128)} %param.29) | copy-start | bytes 1540
  19.2 10.3 %copy-start.3 = (bf16[1024,256]{1,0:T(8,128)(2,1)S(1)}, bf16[1024,256]{1,0:T(8,128)(2,1)}, u32[]{:S(2)}) copy-start(bf16[1024,256]{1,0:T(8,128)(2,1)} %param.30) | copy-start | bytes 1572868
  19.2 10.2 %copy-start.9 = (bf16[32,256]{1,0:T(8,128)(2,1)S(1)}, bf16[32,256]{1,0:T(8,128)(2,1)}, u32[]{:S(2)}) copy-start(bf16[32,256]{1,0:T(8,128)(2,1)} %param.17) | copy-start | bytes 49156
  20.9 41.9 %copy-start.12 = (f32[256]{0:T(256)S(1)}, f32[256]{0:T(256)}, u32[]{:S(2)}) copy-start(f32[256]{0:T(256)} %param.31) | copy-start | bytes 3076
  21.2 41.7 %copy-start.7 = (bf16[256,256]{1,0:T(8,128)(2,1)S(1)}, bf16[256,256]{1,0:T(8,128)(2,1)}, u32[]{:S(2)}) copy-start(bf16[256,256]{1,0:T(8,128)(2,1)} %param.32) | copy-start | bytes 393220
  57.0 10.6 %all-to-all-start.4 = ((f32[8,1,1024]{2,1,0:T(1,128)}), f32[8,1,1024]{2,1,0:T(1,128)S(1)}, u32[]{:S(2)}, u32[]{:S(2)}) async-start(f32[8,1,1024]{2,1,0:T(1,128)} %broadcast_in_dim.16), calls=%async_computation.4 | async-start | bytes 65536 | tf_op jit(solution)/shard_map/all_to_all | solution.py:16
  62.9 31.0 %copy-start.8 = (bf16[256,256]{1,0:T(8,128)(2,1)S(1)}, bf16[256,256]{1,0:T(8,128)(2,1)}, u32[]{:S(2)}) copy-start(bf16[256,256]{1,0:T(8,128)(2,1)} %param.33) | copy-start | bytes 393220
  67.5 13.5 %all-to-all-start.3 = ((bf16[8,1024,32]{1,2,0:T(8,128)(2,1)}), bf16[8,1024,32]{1,2,0:T(8,128)(2,1)S(1)}, u32[]{:S(2)}, u32[]{:S(2)}) async-start(bf16[8,1024,32]{1,2,0:T(8,128)(2,1)} %bitcast.19), calls=%async_computation.3 | async-start | bytes 1048576 | tf_op jit(solution)/shard_map/all_to_all | solution.py:38
where the time goes:
time: 116 us; the launch traced here: 115 us
  blocking collectives  66.8 us (58%)
  starting transfers between devices  16.4 us (14%)
  waiting for transfers between devices  16.1 us (14%)
  matrix products  7.53 us (6%)
  local copies, waits for them, and re-layouts  4.38 us (4%)
  other arithmetic  2.28 us (2%)
    all_to_all x3, blocking collectives, from_everyone(): return lax.all_to_all(copies, axis, split_axis=0, concat_axis=0, tiled=True)  47.2 us
    all_to_all x1, blocking collectives, sum_at_owner(): lax.all_to_all(blocks, axis, split_axis=0, concat_axis=0, tiled=True)  19.6 us
    all_to_all x2, starting transfers between devices, from_everyone(): return lax.all_to_all(copies, axis, split_axis=0, concat_axis=0, tiled=True)  12.3 us
    all_to_all x1, waiting for transfers between devices, sum_at_owner(): lax.all_to_all(blocks, axis, split_axis=0, concat_axis=0, tiled=True)  9.34 us
    all_to_all x2, waiting for transfers between devices, from_everyone(): return lax.all_to_all(copies, axis, split_axis=0, concat_axis=0, tiled=True)  6.8 us
    all_to_all x1, starting transfers between devices, sum_at_owner(): lax.all_to_all(blocks, axis, split_axis=0, concat_axis=0, tiled=True)  4.13 us
    broadcast_in_dim x6, local copies, waits for them, and re-layouts, from_everyone(): copies = jnp.broadcast_to(value, (lax.axis_size(axis), *value.shape))  2.32 us
  transfers between devices with their start and end apart: 3, of which 3 were waited for; matrix products, arithmetic and copies ran while one was open for 3% of the time, Pallas kernels for 0%

commit v1 on v0

v1 whole, which is shorter than its diff:
```python
import jax
import jax.numpy as jnp
from jax import lax
from jax.experimental import pallas as pl
from jax.experimental.pallas import tpu as pltpu
from jax.sharding import PartitionSpec as P

D = 2048
DK = 128
EPS = 1e-06
XN = 4
ZN = 8
YN = 4
TN = 8
ROWS = 32
DB = D // TN
SUB = ROWS // TN
FB = 256
ZORD = (0, 1, 7, 2, 6, 3, 5, 4)
ZPOS = tuple(ZORD.index(o) for o in range(ZN))
TPO = ((2, 0), (2, 1), (1, 0), (1, 1), (3, 0), (3, 1), (0, 1))
GROUPS = ZN // 2
F32 = jnp.float32
BF16 = jnp.bfloat16
MESH = pl.DeviceIdType.MESH


def remote(src, dst, send_sem, recv_sem, kv, tp):
    return pltpu.make_async_remote_copy(
        src_ref=src,
        dst_ref=dst,
        send_sem=send_sem,
        recv_sem=recv_sem,
        device_id={"kv": kv, "tp": tp},
        device_id_type=MESH,
    )


def await_bytes(ref, sem):
    pltpu.make_async_copy(ref, ref, sem).wait()


def kernel(
    tok_h, mem_h, nrm_h, stab_h, ng_h, qw_h, kw_h, vw_h, ow_h, ig_h, fg_h, fb_h, mg_h, pw_h, gain_h, up_h, dn_h,
    out_ref, memn_h, nrmn_ref, stabn_ref,
    tk, mem, nrm, stab, ng, qkvo, ig, fg, fb, mg, pw, gains, upb, dnb,
    nb, qf, colrow, colmat, mx, secf, seg, xbuf, xs, os, rsx_s, rsx_r, own, zs, fin, of,
    lsem, tok_s, tok_r, gain_s, gain_r, mix_s, mix_r, w_s, w_r, az_s, az_r, xf_s, xf_r, rx_s, rx_r, fi_s, fi_r,
    zready,
):
    kv = lax.axis_index("kv")
    t = lax.axis_index("tp")
    z, x = kv // XN, kv % XN
    y, c = t // 2, t % 2

    def zx(dz, dx):
        return ((z + dz) % ZN) * XN + (x + dx) % XN

    def tp_at(dy, dc):
        return ((y + dy) % YN) * 2 + (c + dc) % 2

    pending = []

    def send(src, dst, ssem, rsem, kv_to, tp_to):
        remote(src, dst, ssem, rsem, kv_to, tp_to).start()
        pending.append((src, ssem))

    lane_t = pl.ds(pl.multiple_of(t * DB, DB), DB)
    lane_h = pl.ds(pl.multiple_of(t * DK, DK), DK)
    row_t = lane_t

    loads = {}

    def load(name, src, dst):
        k = len(loads)
        loads[name] = pltpu.make_async_copy(src, dst, lsem.at[k])
        loads[name].start()

    load("tok", tok_h, tk.at[:, lane_t])
    load("gain", gain_h, gains.at[:, lane_t])
    load("up", up_h, upb.at[row_t])
    load("dn", dn_h, dnb.at[t])
    load("ng", ng_h, ng)
    for k, (name, w) in enumerate((("q", qw_h), ("k", kw_h), ("v", vw_h), ("o", ow_h))):
        load(name, w, qkvo.at[:, DK * k : DK * (k + 1)])
    load("ig", ig_h, ig)
    load("fg", fg_h, fg)
    load("fb", fb_h, fb)
    load("stab", stab_h, stab)
    load("nrm", nrm_h, nrm)
    load("mem", mem_h, mem)
    load("mg", mg_h, mg)
    load("pw", pw_h, pw)

    barrier = pltpu.get_barrier_semaphore()
    for dy, dc in TPO:
        pl.semaphore_signal(barrier, inc=1, device_id={"kv": kv, "tp": tp_at(dy, dc)}, device_id_type=MESH)
    for dx in range(1, XN):
        pl.semaphore_signal(barrier, inc=1, device_id={"kv": zx(0, dx), "tp": t}, device_id_type=MESH)
    for dz in range(1, ZN):
        pl.semaphore_signal(barrier, inc=1, device_id={"kv": zx(dz, 0), "tp": t}, device_id_type=MESH)
    pl.semaphore_wait(barrier, 7 + (XN - 1) + (ZN - 1))
    for dz in range(1, ZN):
        pl.semaphore_signal(zready, inc=1, device_id={"kv": zx(dz, 0), "tp": t}, device_id_type=MESH)

    loads["tok"].wait()
    for k, (dy, dc) in enumerate(TPO):
        send(tk.at[:, lane_t], tk.at[:, lane_t], tok_s.at[k], tok_r.at[k], kv, tp_at(dy, dc))
    loads["gain"].wait()
    for k, (dy, dc) in enumerate(TPO):
        send(gains.at[:, lane_t], gains.at[:, lane_t], gain_s.at[k], gain_r.at[k], kv, tp_at(dy, dc))

    def w_slot(m, dy, dc):
        s = tp_at(dy, dc)
        return upb.at[pl.ds(pl.multiple_of(s * DB, DB), DB)] if m == 0 else dnb.at[s]

    loads["up"].wait()
    send(w_slot(0, 0, 0), w_slot(0, 0, 0), w_s.at[0, 0], w_r.at[0, 0], kv, tp_at(1, 0))
    send(w_slot(0, 0, 0), w_slot(0, 0, 0), w_s.at[0, 1], w_r.at[0, 1], kv, tp_at(3, 0))
    send(w_slot(0, 0, 0), w_slot(0, 0, 0), w_s.at[0, 3], w_r.at[0, 3], kv, tp_at(0, 1))
    loads["dn"].wait()
    send(w_slot(1, 0, 0), w_slot(1, 0, 0), w_s.at[1, 0], w_r.at[1, 0], kv, tp_at(1, 0))
    send(w_slot(1, 0, 0), w_slot(1, 0, 0), w_s.at[1, 1], w_r.at[1, 1], kv, tp_at(3, 0))
    send(w_slot(1, 0, 0), w_slot(1, 0, 0), w_s.at[1, 3], w_r.at[1, 3], kv, tp_at(0, 1))

    for name in ("ng", "q", "k", "v", "o", "ig", "fg", "fb", "stab", "nrm"):
        loads[name].wait()
    for k, (dy, dc) in enumerate(TPO):
        s = tp_at(-dy, -dc)
        await_bytes(tk.at[:, pl.ds(pl.multiple_of(s * DB, DB), DB)], tok_r.at[k])
    rows = tk[...].astype(F32)
    scale_one = lax.rsqrt(jnp.sum(rows * rows, axis=-1, keepdims=True) * (1.0 / D) + EPS)
    nb[...] = (rows * scale_one * ng[...]).astype(BF16)
    proj4 = jnp.dot(nb[...], qkvo[...], preferred_element_type=F32).astype(BF16).astype(F32)
    query = proj4[:, :DK]
    keys = proj4[:, DK : 2 * DK] * DK ** (-0.5)
    values = proj4[:, 2 * DK : 3 * DK]
    gate_out = proj4[:, 3 * DK :]
    qf[...] = query

    contract = (((1,), (1,)), ((), ()))
    all_in = lax.dot_general(nb[...], ig[...], contract, preferred_element_type=F32)
    all_forget = lax.dot_general(nb[...], fg[...], contract, preferred_element_type=F32) + fb[...]
    head = lax.broadcasted_iota(jnp.int32, (ROWS, TN), 1) == t
    input_log = jnp.sum(jnp.where(head, all_in, 0.0), axis=1, keepdims=True)
    raw = jnp.sum(jnp.where(head, all_forget, 0.0), axis=1, keepdims=True)
    forget_log = jnp.minimum(raw, 0.0) - jnp.log1p(jnp.exp(-jnp.abs(raw)))
    diag = lax.broadcasted_iota(jnp.int32, (ROWS, ROWS), 0) == lax.broadcasted_iota(jnp.int32, (ROWS, ROWS), 1)
    stab_col = jnp.sum(jnp.where(diag, jnp.broadcast_to(stab[...], (ROWS, ROWS)), 0.0), axis=1, keepdims=True)
    stab_new = jnp.maximum(forget_log + stab_col, input_log)
    keep = jnp.exp(forget_log + stab_col - stab_new)
    admit = jnp.exp(input_log - stab_new)
    normalizer_new = keep * nrm[...] + admit * keys
    denom = jnp.sum(normalizer_new * query, axis=1, keepdims=True)
    key_query = jnp.sum(keys * query, axis=1, keepdims=True)

    loads["mem"].wait()
    lane = lax.broadcasted_iota(jnp.int32, (DK, DK), 1)

    def read_memory(b, acc):
        part = jnp.sum(mem[b] * qf[pl.ds(b, 1), :], axis=1, keepdims=True)
        return jnp.where(lane == b, part, acc)

    read = lax.fori_loop(0, ROWS, read_memory, jnp.zeros((DK, DK), F32), unroll=4)
    memory_query = read.T[:ROWS, :]
    numer = keep * memory_query + (admit * key_query) * values
    cell = numer / jnp.maximum(jnp.abs(denom), 1.0)
    loads["mg"].wait()
    mx[:, lane_h] = (cell * mg[...] * jax.nn.sigmoid(gate_out)).astype(BF16)
    for k, (dy, dc) in enumerate(TPO):
        send(mx.at[:, lane_h], mx.at[:, lane_h], mix_s.at[k], mix_r.at[k], kv, tp_at(dy, dc))

    nrmn_ref[...] = normalizer_new
    stabn_ref[...] = jnp.sum(
        jnp.where(diag, jnp.broadcast_to(stab_new, (ROWS, ROWS)), 0.0), axis=0, keepdims=True
    )
    colrow[0] = jnp.broadcast_to(keep, (ROWS, DK))
    colrow[1] = keys
    colmat[:ROWS, :] = admit * values
    colmat[ROWS:, :] = jnp.zeros((DK - ROWS, DK), F32)
    admitted = colmat[...].T

    def write_memory(b, carry):
        column = jnp.sum(jnp.where(lane == b, admitted, 0.0), axis=1, keepdims=True)
        mem[b] = colrow[0, pl.ds(b, 1), :] * mem[b] + column * colrow[1, pl.ds(b, 1), :]
        return carry

    lax.fori_loop(0, ROWS, write_memory, 0, unroll=4)
    store_mem = pltpu.make_async_copy(mem, memn_h, lsem.at[len(loads)])
    store_mem.start()

    loads["pw"].wait()
    for k, (dy, dc) in enumerate(TPO):
        s = tp_at(-dy, -dc)
        await_bytes(mx.at[:, pl.ds(pl.multiple_of(s * DK, DK), DK)], mix_r.at[k])
    projected = jnp.dot(mx[...], pw[...], preferred_element_type=F32)
    second = (tk[:, lane_t].astype(F32) + projected).astype(BF16).astype(F32)
    secf[...] = second
    for s in range(TN):
        seg[s] = secf[SUB * s : SUB * (s + 1), :].astype(BF16)

    pl.semaphore_wait(zready, ZN - 1)
    own_seg = pltpu.make_async_copy(seg.at[t], xbuf.at[0, 0, t], az_r.at[0])
    own_seg.start()
    for dz in (4, 3, 5, 2, 6, 1, 7, 0):
        there = ZPOS[(-dz) % ZN]
        for dy, dc in TPO if dz == 0 else TPO + ((0, 0),):
            s = tp_at(dy, dc)
            remote(
                seg.at[s], xbuf.at[0, there, t], az_s.at[ZPOS[dz]], az_r.at[there], zx(dz, 0), s
            ).start()

    def relay(m, k, dy, forward):
        slot = w_slot(m, dy, 0)
        await_bytes(slot, w_r.at[m, k])
        if forward is not None:
            send(slot, slot, w_s.at[m, 2], w_r.at[m, 2], kv, tp_at(forward, 0))
        send(slot, slot, w_s.at[m, 4 + k], w_r.at[m, 4 + k], kv, tp_at(0, 1))

    relay(0, 0, 3, 1)
    relay(1, 1, 1, 3)
    relay(0, 1, 1, None)
    relay(1, 0, 3, None)

    for g in range(GROUPS):
        for p in (2 * g, 2 * g + 1):
            await_bytes(xbuf.at[0, p], az_r.at[p])
        pair = pl.ds(2 * g, 2)
        for dx in range(1, XN):
            send(
                xbuf.at[0, pair], xbuf.at[(-dx) % XN, pair],
                xf_s.at[dx - 1, g], xf_r.at[(-dx) % XN - 1, g], zx(0, dx), t,
            )

    relay(0, 2, 2, None)
    relay(1, 2, 2, None)
    for k, (dy, dc) in enumerate(TPO):
        s = tp_at(-dy, -dc)
        await_bytes(gains.at[:, pl.ds(pl.multiple_of(s * DB, DB), DB)], gain_r.at[k])
    for m in range(2):
        for k, dy in ((3, 0), (4, 3), (5, 1), (6, 2)):
            await_bytes(w_slot(m, dy, 1), w_r.at[m, k])

    def mixer(g):
        for dx in range(1, XN):
            await_bytes(xbuf.at[dx, pl.ds(2 * g, 2)], xf_r.at[dx - 1, g])
        for i in range(2 * XN):
            dx, p = i // 2, 2 * g + i % 2
            block = xbuf[dx, p].astype(F32)
            for j in range(TN):
                xs[SUB * i : SUB * (i + 1), DB * j : DB * (j + 1)] = block[j]
        sec = xs[...]
        scale_two = lax.rsqrt(jnp.sum(sec * sec, axis=-1, keepdims=True) * (1.0 / D) + EPS)
        scaled = (sec * gains[...]).astype(BF16)
        preact = jnp.dot(scaled, upb[...], preferred_element_type=F32)
        hidden = jnp.square(jnp.maximum(preact * scale_two, 0.0)).astype(BF16)
        for j in range(TN):
            os[:, DB * j : DB * (j + 1)] = jnp.dot(hidden, dnb[j], preferred_element_type=F32)
        for i in range(2 * XN):
            dx, p = i // 2, 2 * g + i % 2
            for j in range(TN):
                block = os[SUB * i : SUB * (i + 1), DB * j : DB * (j + 1)]
                if dx == 0:
                    own[p, j] = block
                else:
                    rsx_s[dx - 1, p, j] = block.astype(BF16)
        pair = pl.ds(2 * g, 2)
        for dx in range(1, XN):
            send(
                rsx_s.at[dx - 1, pair], rsx_r.at[(-dx) % XN - 1, pair],
                rx_s.at[dx - 1, g], rx_r.at[(-dx) % XN - 1, g], zx(0, dx), t,
            )

    def sum_x(g):
        pair = pl.ds(2 * g, 2)
        for dx in range(1, XN):
            await_bytes(rsx_r.at[dx - 1, pair], rx_r.at[dx - 1, g])
        for p in (2 * g, 2 * g + 1):
            total = own[p]
            for dx in range(1, XN):
                total += rsx_r[dx - 1, p].astype(F32)
            zs[p] = total.astype(BF16)
            dz = ZORD[p]
            there = ZPOS[(-dz) % ZN]
            if dz == 0:
                pltpu.make_async_copy(zs.at[p, t], fin.at[0, t], fi_r.at[0]).start()
            for dy, dc in TPO if dz == 0 else TPO + ((0, 0),):
                s = tp_at(dy, dc)
                remote(
                    zs.at[p, s], fin.at[there, t], fi_s.at[p], fi_r.at[there], zx(dz, 0), s
                ).start()

    mixer(0)
    for g in range(1, GROUPS):
        mixer(g)
        sum_x(g - 1)
    sum_x(GROUPS - 1)

    total = jnp.zeros((TN, SUB, DB), F32)
    for p in range(ZN):
        await_bytes(fin.at[p], fi_r.at[p])
        total += fin[p].astype(F32)
    for s in range(TN):
        of[SUB * s : SUB * (s + 1), :] = total[s]
    out_ref[...] = (secf[...] + of[...]).astype(BF16)

    for src, sem in pending:
        await_bytes(src, sem)
    for p in range(ZN):
        count = TN - 1 if p == 0 else TN
        await_bytes(seg.at[pl.ds(0, count)], az_s.at[p])
        await_bytes(zs.at[p, pl.ds(0, count)], fi_s.at[p])
    store_mem.wait()


def per_device(
    tokens, memory, normalizer, stabilizer, norm_gain, query_weight, key_weight, value_weight, outgate_weight,
    input_gate_weight, forget_gate_weight, forget_bias, memory_gain, proj_weight, ffn_gain, up_weight, down_weight,
):
    hbm = pl.BlockSpec(memory_space=pl.ANY)
    vmem = pl.BlockSpec(memory_space=pltpu.VMEM)
    dma = pltpu.SemaphoreType.DMA
    layer_out, memory_new, normalizer_new, stab_new = pl.pallas_call(
        kernel,
        out_shape=(
            jax.ShapeDtypeStruct((ROWS, DB), BF16),
            jax.ShapeDtypeStruct((ROWS, DK, DK), F32),
            jax.ShapeDtypeStruct((ROWS, DK), F32),
            jax.ShapeDtypeStruct((1, ROWS), F32),
        ),
        in_specs=[hbm] * 17,
        out_specs=(vmem, hbm, vmem, vmem),
        scratch_shapes=[
            pltpu.VMEM((ROWS, D), BF16),
            pltpu.VMEM((ROWS, DK, DK), F32),
            pltpu.VMEM((ROWS, DK), F32),
            pltpu.VMEM((1, ROWS), F32),
            pltpu.VMEM((1, D), F32),
            pltpu.VMEM((D, 4 * DK), BF16),
            pltpu.VMEM((TN, D), BF16),
            pltpu.VMEM((TN, D), BF16),
            pltpu.VMEM((1, TN), F32),
            pltpu.VMEM((1, DK), F32),
            pltpu.VMEM((TN * DK, DB), BF16),
            pltpu.VMEM((1, D), F32),
            pltpu.VMEM((D, FB), BF16),
            pltpu.VMEM((TN, FB, DB), BF16),
            pltpu.VMEM((ROWS, D), BF16),
            pltpu.VMEM((ROWS, DK), F32),
            pltpu.VMEM((2, ROWS, DK), F32),
            pltpu.VMEM((DK, DK), F32),
            pltpu.VMEM((ROWS, TN * DK), BF16),
            pltpu.VMEM((ROWS, DB), F32),
            pltpu.VMEM((TN, SUB, DB), BF16),
            pltpu.VMEM((XN, ZN, TN, SUB, DB), BF16),
            pltpu.VMEM((ROWS, D), F32),
            pltpu.VMEM((ROWS, D), F32),
            pltpu.VMEM((XN - 1, ZN, TN, SUB, DB), BF16),
            pltpu.VMEM((XN - 1, ZN, TN, SUB, DB), BF16),
            pltpu.VMEM((ZN, TN, SUB, DB), F32),
            pltpu.VMEM((ZN, TN, SUB, DB), BF16),
            pltpu.VMEM((ZN, TN, SUB, DB), BF16),
            pltpu.VMEM((ROWS, DB), F32),
            dma((18,)),
            dma((7,)), dma((7,)),
            dma((7,)), dma((7,)),
            dma((7,)), dma((7,)),
            dma((2, 7)), dma((2, 7)),
            dma((ZN,)), dma((ZN,)),
            dma((XN - 1, GROUPS)), dma((XN - 1, GROUPS)),
            dma((XN - 1, GROUPS)), dma((XN - 1, GROUPS)),
            dma((ZN,)), dma((ZN,)),
            pltpu.SemaphoreType.REGULAR,
        ],
        compiler_params=pltpu.CompilerParams(
            collective_id=0, has_side_effects=True, vmem_limit_bytes=40 * 1024 * 1024
        ),
        name="layer",
    )(
        tokens,
        memory.reshape(ROWS, DK, DK),
        normalizer.reshape(ROWS, DK),
        stabilizer.T,
        norm_gain.reshape(1, D),
        query_weight, key_weight, value_weight, outgate_weight,
        input_gate_weight.T,
        forget_gate_weight.T,
        forget_bias.reshape(1, TN),
        memory_gain.reshape(1, DK),
        proj_weight,
        ffn_gain.reshape(1, DB),
        up_weight,
        down_weight,
    )
    return (
        layer_out,
        memory_new.reshape(ROWS, 1, DK, DK),
        normalizer_new.reshape(ROWS, 1, DK),
        stab_new.T,
    )


def solution(mesh):
    placed = (
        P("kv", "tp"),
        P("kv", "tp", None, None),
        P("kv", "tp", None),
        P("kv", "tp"),
        P(),
        P(None, "tp"),
        P(None, "tp"),
        P(None, "tp"),
        P(None, "tp"),
        P(),
        P(),
        P(),
        P("tp"),
        P(None, "tp"),
        P("tp"),
        P("tp", "kv"),
        P("kv", "tp"),
    )
    outs = (P("kv", "tp"), P("kv", "tp", None, None), P("kv", "tp", None), P("kv", "tp"))
    return jax.shard_map(per_device, mesh=mesh, in_specs=placed, out_specs=outs, check_vma=False)
```

time: 116 us -> 69.7 us (0.60)
  blocking collectives: 66.8 us -> 0 us
  Pallas kernels: 0 us -> 50.3 us
  starting transfers between devices: 16.4 us -> 0 us
  waiting for transfers between devices: 16.1 us -> 0 us
  local copies, waits for them, and re-layouts: 4.38 us -> 17.9 us
  matrix products: 7.53 us -> 0 us
  other arithmetic: 2.28 us -> 0 us
    all_to_all x4 -> x0, blocking collectives: 66.8 us -> none  [the longest x3 47.2 us: from_everyone(): return lax.all_to_all(copies, axis, split_axis=0, concat_axis=0, tiled=True)]
    pallas_call x0 -> x1, Pallas kernels: none -> 50.3 us  [per_device(): pl.pallas_call(kernel, out_shape=(jax.ShapeDtypeStruct((ROWS, DB), BF16),...]
    unnamed x30 -> x38, local copies, waits for them, and re-layouts: 0.1 us -> 17.9 us
    all_to_all x3 -> x0, starting transfers between devices: 16.4 us -> none  [the longest x2 12.3 us: from_everyone(): return lax.all_to_all(copies, axis, split_axis=0, concat_axis=0, tiled=True)]
    all_to_all x3 -> x0, waiting for transfers between devices: 16.1 us -> none  [the longest x1 9.34 us: sum_at_owner(): lax.all_to_all(blocks, axis, split_axis=0, concat_axis=0, tiled=True)]
    dot_general x10 -> x0, matrix products: 7.53 us -> none  [the longest x1 1.73 us: per_device(): jnp.einsum('bhed,bhd->bhe', memory_new, query_f, precision=lax.Precision....]
    broadcast_in_dim x6 -> x0, local copies, waits for them, and re-layouts: 2.32 us -> none  [from_everyone(): copies = jnp.broadcast_to(value, (lax.axis_size(axis), *value.shape))]
    dynamic_slice x1 -> x0, local copies, waits for them, and re-layouts: 1.24 us -> none  [per_device(): bias_here = lax.dynamic_slice_in_dim(forget_bias, first_head, heads_here, 0)]
  transfers between devices with their start and end apart: 3 -> 0, of which waited for: 3 -> 0; matrix products, arithmetic and copies ran while one was open for 3% -> 0% of each run, Pallas kernels for 0% -> 0%
where the time goes in v1:
time: 69.7 us; the launch traced here: 68.9 us
  Pallas kernels  50.3 us (72%)
  local copies, waits for them, and re-layouts  17.9 us (26%)
    pallas_call x1, Pallas kernels, per_device(): pl.pallas_call(kernel, out_shape=(jax.ShapeDtypeStruct((ROWS, DB), BF16),...  50.3 us
    unnamed x38, local copies, waits for them, and re-layouts  17.9 us

profile of v1, /device:TPU:1, one launch (start us, length us, event | category | flops | bytes accessed | tf_op | source)
XLA Modules:
  0.0 68.9 jit_solution(1907058581268137843)
XLA Ops:
  0.6 0.0 copy-start
  0.6 1.6 %copy-done = f32[32,1,128,128]{3,2,1,0:T(8,128)S(1)} copy-done((f32[32,1,128,128]{3,2,1,0:T(8,128)S(1)}, f32[32,1,128,128]{3,2,1,0:T(8,128)}, u32[]{:S(2)}) %copy-start) | copy-done | bytes 2097176
  2.2 0.0 copy-start.1
  2.2 1.0 %copy-done.1 = bf16[2048,128]{1,0:T(8,128)(2,1)S(1)} copy-done((bf16[2048,128]{1,0:T(8,128)(2,1)S(1)}, bf16[2048,128]{1,0:T(8,128)(2,1)}, u32[]{:S(2)}) %copy-start.1) | copy-done | bytes 524312
  3.3 0.0 copy-start.2
  3.3 1.0 %copy-done.2 = bf16[2048,128]{1,0:T(8,128)(2,1)S(1)} copy-done((bf16[2048,128]{1,0:T(8,128)(2,1)S(1)}, bf16[2048,128]{1,0:T(8,128)(2,1)}, u32[]{:S(2)}) %copy-start.2) | copy-done | bytes 524312
  4.3 0.0 copy-start.3
  4.3 1.0 %copy-done.3 = bf16[2048,128]{1,0:T(8,128)(2,1)S(1)} copy-done((bf16[2048,128]{1,0:T(8,128)(2,1)S(1)}, bf16[2048,128]{1,0:T(8,128)(2,1)}, u32[]{:S(2)}) %copy-start.3) | copy-done | bytes 524312
  5.4 0.0 copy-start.4
  5.4 1.0 %copy-done.4 = bf16[2048,128]{1,0:T(8,128)(2,1)S(1)} copy-done((bf16[2048,128]{1,0:T(8,128)(2,1)S(1)}, bf16[2048,128]{1,0:T(8,128)(2,1)}, u32[]{:S(2)}) %copy-start.4) | copy-done | bytes 524312
  6.4 0.0 copy-start.5
  6.4 1.0 %copy-done.5 = bf16[1024,256]{1,0:T(8,128)(2,1)S(1)} copy-done((bf16[1024,256]{1,0:T(8,128)(2,1)S(1)}, bf16[1024,256]{1,0:T(8,128)(2,1)}, u32[]{:S(2)}) %copy-start.5) | copy-done | bytes 524312
  7.4 0.0 copy-start.6
  7.4 0.9 %copy-done.6 = bf16[256,256]{1,0:T(8,128)(2,1)S(1)} copy-done((bf16[256,256]{1,0:T(8,128)(2,1)S(1)}, bf16[256,256]{1,0:T(8,128)(2,1)}, u32[]{:S(2)}) %copy-start.6) | copy-done | bytes 131096
  8.3 0.0 copy-start.7
  8.3 0.9 %copy-done.7 = bf16[256,256]{1,0:T(8,128)(2,1)S(1)} copy-done((bf16[256,256]{1,0:T(8,128)(2,1)S(1)}, bf16[256,256]{1,0:T(8,128)(2,1)}, u32[]{:S(2)}) %copy-start.7) | copy-done | bytes 131096
  9.3 0.0 copy-start.8
  9.3 0.8 %copy-done.8 = bf16[2048,8]{0,1:T(8,128)(2,1)S(1)} copy-done((bf16[2048,8]{0,1:T(8,128)(2,1)S(1)}, bf16[2048,8]{0,1:T(8,128)(2,1)}, u32[]{:S(2)}) %copy-start.8) | copy-done | bytes 32792
  10.0 0.0 copy-start.9
  10.0 0.8 %copy-done.9 = bf16[2048,8]{0,1:T(8,128)(2,1)S(1)} copy-done((bf16[2048,8]{0,1:T(8,128)(2,1)S(1)}, bf16[2048,8]{0,1:T(8,128)(2,1)}, u32[]{:S(2)}) %copy-start.9) | copy-done | bytes 32792
  10.8 0.0 copy-start.10
  10.8 0.7 %copy-done.10 = bf16[32,256]{1,0:T(8,128)(2,1)S(1)} copy-done((bf16[32,256]{1,0:T(8,128)(2,1)S(1)}, bf16[32,256]{1,0:T(8,128)(2,1)}, u32[]{:S(2)}) %copy-start.10) | copy-done | bytes 16408
  11.5 0.0 copy-start.11
  11.5 0.7 %copy-done.11 = f32[32,1,128]{2,1,0:T(1,128)S(1)} copy-done((f32[32,1,128]{2,1,0:T(1,128)S(1)}, f32[32,1,128]{2,1,0:T(1,128)}, u32[]{:S(2)}) %copy-start.11) | copy-done | bytes 16408
  12.2 0.0 copy-start.12
  12.2 0.7 %copy-done.12 = f32[2048]{0:T(1024)S(1)} copy-done((f32[2048]{0:T(1024)S(1)}, f32[2048]{0:T(1024)}, u32[]{:S(2)}) %copy-start.12) | copy-done | bytes 8216
  12.9 0.0 copy-start.13
  12.9 0.7 copy-done.13
  13.6 0.0 copy-start.14
  13.6 0.7 copy-done.14
  14.2 0.0 copy-start.15
  14.2 0.7 copy-done.15
  14.9 0.0 copy-start.16
  14.9 0.7 copy-done.16
  15.5 50.3 %layer.1 = (bf16[32,256]{1,0:T(8,128)(2,1)S(1)}, f32[32,128,128]{2,1,0:T(8,128)S(1)}, f32[32,128]{1,0:T(8,128)S(1)}, f32[1,32]{1,0:T(1,128)S(1)}) custom-call(bf16[32,256]{1,0:T(8,128)(2,1)S(1)} %copy-done.10, f32[32,128,128]{2,1,0:T(8,128)S(1)} %bitcast.16, f32[32,128]{1,0:T(8,128)S(1)} %bitcast.20, f32[1,32]{1,0:T(1,128)S(1)} %bitcast.24, ...), custom_call_target="tpu_custom_call" | custom-call | tf_op jit(solution)/shard_map/layer/pallas_call | solution.py:323
  65.9 0.6 copy.27
  66.5 1.3 %copy.28 = f32[32,1,128,128]{3,2,1,0:T(8,128)} copy(f32[32,1,128,128]{3,2,1,0:T(8,128)S(1)} %bitcast.17) | data formatting | bytes 4194304
  67.8 0.6 copy.29
  68.4 0.5 copy.30
Async XLA Ops:
  0.6 1.6 %copy-start = (f32[32,1,128,128]{3,2,1,0:T(8,128)S(1)}, f32[32,1,128,128]{3,2,1,0:T(8,128)}, u32[]{:S(2)}) copy-start(f32[32,1,128,128]{3,2,1,0:T(8,128)} %param.18) | copy-start | bytes 6291460
  2.2 1.0 %copy-start.1 = (bf16[2048,128]{1,0:T(8,128)(2,1)S(1)}, bf16[2048,128]{1,0:T(8,128)(2,1)}, u32[]{:S(2)}) copy-start(bf16[2048,128]{1,0:T(8,128)(2,1)} %qw_h.1) | copy-start | bytes 1572868
  3.3 1.0 %copy-start.2 = (bf16[2048,128]{1,0:T(8,128)(2,1)S(1)}, bf16[2048,128]{1,0:T(8,128)(2,1)}, u32[]{:S(2)}) copy-start(bf16[2048,128]{1,0:T(8,128)(2,1)} %kw_h.1) | copy-start | bytes 1572868
  4.3 1.0 %copy-start.3 = (bf16[2048,128]{1,0:T(8,128)(2,1)S(1)}, bf16[2048,128]{1,0:T(8,128)(2,1)}, u32[]{:S(2)}) copy-start(bf16[2048,128]{1,0:T(8,128)(2,1)} %vw_h.1) | copy-start | bytes 1572868
  5.4 1.0 %copy-start.4 = (bf16[2048,128]{1,0:T(8,128)(2,1)S(1)}, bf16[2048,128]{1,0:T(8,128)(2,1)}, u32[]{:S(2)}) copy-start(bf16[2048,128]{1,0:T(8,128)(2,1)} %ow_h.1) | copy-start | bytes 1572868
  6.4 1.0 %copy-start.5 = (bf16[1024,256]{1,0:T(8,128)(2,1)S(1)}, bf16[1024,256]{1,0:T(8,128)(2,1)}, u32[]{:S(2)}) copy-start(bf16[1024,256]{1,0:T(8,128)(2,1)} %pw_h.1) | copy-start | bytes 1572868
  7.4 0.9 %copy-start.6 = (bf16[256,256]{1,0:T(8,128)(2,1)S(1)}, bf16[256,256]{1,0:T(8,128)(2,1)}, u32[]{:S(2)}) copy-start(bf16[256,256]{1,0:T(8,128)(2,1)} %up_h.1) | copy-start | bytes 393220
  8.3 0.9 %copy-start.7 = (bf16[256,256]{1,0:T(8,128)(2,1)S(1)}, bf16[256,256]{1,0:T(8,128)(2,1)}, u32[]{:S(2)}) copy-start(bf16[256,256]{1,0:T(8,128)(2,1)} %dn_h.1) | copy-start | bytes 393220
  9.3 0.8 %copy-start.8 = (bf16[2048,8]{0,1:T(8,128)(2,1)S(1)}, bf16[2048,8]{0,1:T(8,128)(2,1)}, u32[]{:S(2)}) copy-start(bf16[2048,8]{0,1:T(8,128)(2,1)} %param.26) | copy-start | bytes 98308
  10.0 0.8 %copy-start.9 = (bf16[2048,8]{0,1:T(8,128)(2,1)S(1)}, bf16[2048,8]{0,1:T(8,128)(2,1)}, u32[]{:S(2)}) copy-start(bf16[2048,8]{0,1:T(8,128)(2,1)} %param.27) | copy-start | bytes 98308
  10.8 0.7 %copy-start.10 = (bf16[32,256]{1,0:T(8,128)(2,1)S(1)}, bf16[32,256]{1,0:T(8,128)(2,1)}, u32[]{:S(2)}) copy-start(bf16[32,256]{1,0:T(8,128)(2,1)} %tok_h.1) | copy-start | bytes 49156
  11.5 0.7 %copy-start.11 = (f32[32,1,128]{2,1,0:T(1,128)S(1)}, f32[32,1,128]{2,1,0:T(1,128)}, u32[]{:S(2)}) copy-start(f32[32,1,128]{2,1,0:T(1,128)} %param.19) | copy-start | bytes 49156
  12.2 0.7 %copy-start.12 = (f32[2048]{0:T(1024)S(1)}, f32[2048]{0:T(1024)}, u32[]{:S(2)}) copy-start(f32[2048]{0:T(1024)} %param.21) | copy-start | bytes 24580
  12.9 0.7 copy-start.13
  13.6 0.7 copy-start.14
  14.2 0.7 copy-start.15
  14.9 0.7 copy-start.16

commit v2 on v1

--- a/solution.py
+++ b/solution.py
@@ -313,23 +313,34 @@
     store_mem.wait()
 
 
+def write_out(*refs):
+    ins, outs, sems = refs[:4], refs[4:8], refs[8]
+    copies = [pltpu.make_async_copy(src, dst, sems.at[k]) for k, (src, dst) in enumerate(zip(ins, outs))]
+    for copy in copies:
+        copy.start()
+    for copy in copies:
+        copy.wait()
+
+
 def per_device(
     tokens, memory, normalizer, stabilizer, norm_gain, query_weight, key_weight, value_weight, outgate_weight,
     input_gate_weight, forget_gate_weight, forget_bias, memory_gain, proj_weight, ffn_gain, up_weight, down_weight,
 ):
-    hbm = pl.BlockSpec(memory_space=pl.ANY)
+    hbm = pl.BlockSpec(memory_space=pltpu.HBM)
+    anywhere = pl.BlockSpec(memory_space=pl.ANY)
     vmem = pl.BlockSpec(memory_space=pltpu.VMEM)
     dma = pltpu.SemaphoreType.DMA
+    outs = (
+        jax.ShapeDtypeStruct((ROWS, DB), BF16),
+        jax.ShapeDtypeStruct((ROWS, DK, DK), F32),
+        jax.ShapeDtypeStruct((ROWS, DK), F32),
+        jax.ShapeDtypeStruct((1, ROWS), F32),
+    )
     layer_out, memory_new, normalizer_new, stab_new = pl.pallas_call(
         kernel,
-        out_shape=(
-            jax.ShapeDtypeStruct((ROWS, DB), BF16),
-            jax.ShapeDtypeStruct((ROWS, DK, DK), F32),
-            jax.ShapeDtypeStruct((ROWS, DK), F32),
-            jax.ShapeDtypeStruct((1, ROWS), F32),
-        ),
+        out_shape=outs,
         in_specs=[hbm] * 17,
-        out_specs=(vmem, hbm, vmem, vmem),
+        out_specs=(vmem, anywhere, vmem, vmem),
         scratch_shapes=[
             pltpu.VMEM((ROWS, D), BF16),
             pltpu.VMEM((ROWS, DK, DK), F32),
@@ -377,21 +388,35 @@
         ),
         name="layer",
     )(
-        tokens,
-        memory.reshape(ROWS, DK, DK),
-        normalizer.reshape(ROWS, DK),
-        stabilizer.T,
-        norm_gain.reshape(1, D),
-        query_weight, key_weight, value_weight, outgate_weight,
-        input_gate_weight.T,
-        forget_gate_weight.T,
-        forget_bias.reshape(1, TN),
-        memory_gain.reshape(1, DK),
-        proj_weight,
-        ffn_gain.reshape(1, DB),
-        up_weight,
-        down_weight,
-    )
+        *(
+            pltpu.with_memory_space_constraint(a, pltpu.HBM)
+            for a in (
+                tokens,
+                memory.reshape(ROWS, DK, DK),
+                normalizer.reshape(ROWS, DK),
+                stabilizer.T,
+                norm_gain.reshape(1, D),
+                query_weight, key_weight, value_weight, outgate_weight,
+                input_gate_weight.T,
+                forget_gate_weight.T,
+                forget_bias.reshape(1, TN),
+                memory_gain.reshape(1, DK),
+                proj_weight,
+                ffn_gain.reshape(1, DB),
+                up_weight,
+                down_weight,
+            )
+        )
+    )
+    layer_out, memory_new, normalizer_new, stab_new = pl.pallas_call(
+        write_out,
+        out_shape=outs,
+        in_specs=[anywhere] * 4,
+        out_specs=(hbm,) * 4,
+        scratch_shapes=[dma((4,))],
+        compiler_params=pltpu.CompilerParams(vmem_limit_bytes=4 * 1024 * 1024),
+        name="write_out",
+    )(layer_out, memory_new, normalizer_new, stab_new)
     return (
         layer_out,
         memory_new.reshape(ROWS, 1, DK, DK),

time: 69.7 us -> 51.7 us (0.74)
  local copies, waits for them, and re-layouts: 17.9 us -> 0 us
    unnamed x38 -> x0, local copies, waits for them, and re-layouts: 17.9 us -> none
    pallas_call x1 -> x2, Pallas kernels: 50.3 us -> 50.9 us  [the longest x1 49.6 us: per_device(): pl.pallas_call(kernel, out_shape=outs, in_specs=[hbm] * 17, out_specs=(vm...]
where the time goes in v2:
time: 51.7 us; the launch traced here: 51.6 us
  Pallas kernels  50.9 us (98%)
  between operations  0.65 us (1%)
    pallas_call x1, Pallas kernels, per_device(): pl.pallas_call(kernel, out_shape=outs, in_specs=[hbm] * 17, out_specs=(vm...  49.6 us
    pallas_call x1, Pallas kernels, per_device(): pl.pallas_call(write_out, out_shape=outs, in_specs=[anywhere] * 4, out_sp...  1.37 us

profile of v2, /device:TPU:1, one launch (start us, length us, event | category | flops | bytes accessed | tf_op | source)
XLA Modules:
  0.0 51.6 jit_solution(17631588378787470672)
XLA Ops:
  0.6 49.6 %layer.1 = (bf16[32,256]{1,0:T(8,128)(2,1)S(1)}, f32[32,128,128]{2,1,0:T(8,128)S(1)}, f32[32,128]{1,0:T(8,128)S(1)}, f32[1,32]{1,0:T(1,128)S(1)}) custom-call(bf16[32,256]{1,0:T(8,128)(2,1)} %tok_h.1, f32[32,128,128]{2,1,0:T(8,128)} %bitcast.16, f32[32,128]{1,0:T(8,128)} %bitcast.19, f32[1,32]{1,0:T(1,128)} %bitcast.22, f32[1,2048]{1,0:T(1,128)} %bitcast.20, ...), custom_call_target="tpu_custom_call" | custom-call | tf_op jit(solution)/shard_map/layer/pallas_call | solution.py:339
  50.2 1.4 %write_out.1 = (bf16[32,256]{1,0:T(8,128)(2,1)}, f32[32,128,128]{2,1,0:T(8,128)}, f32[32,128]{1,0:T(8,128)}, f32[1,32]{1,0:T(1,128)}) custom-call(bf16[32,256]{1,0:T(8,128)(2,1)S(1)} %get-tuple-element.12.refs_0_, f32[32,128,128]{2,1,0:T(8,128)S(1)} %get-tuple-element.13.refs_1_, f32[32,128]{1,0:T(8,128)S(1)} %get-tuple-element.14.refs_2_, ...), custom_call_target="tpu_custom_call" | custom-call | tf_op jit(solution)/shard_map/write_out/pallas_call | solution.py:411

commit v3 on v2

--- a/solution.py
+++ b/solution.py
@@ -16,7 +16,8 @@
 DB = D // TN
 SUB = ROWS // TN
 FB = 256
-ZORD = (0, 1, 7, 2, 6, 3, 5, 4)
+ZORD = (7, 2, 6, 3, 5, 4, 1, 0)
+ZSEND = (0, 1, 7, 2, 6, 3, 5, 4)
 ZPOS = tuple(ZORD.index(o) for o in range(ZN))
 TPO = ((2, 0), (2, 1), (1, 0), (1, 1), (3, 0), (3, 1), (0, 1))
 GROUPS = ZN // 2
@@ -118,10 +119,6 @@
     send(w_slot(0, 0, 0), w_slot(0, 0, 0), w_s.at[0, 0], w_r.at[0, 0], kv, tp_at(1, 0))
     send(w_slot(0, 0, 0), w_slot(0, 0, 0), w_s.at[0, 1], w_r.at[0, 1], kv, tp_at(3, 0))
     send(w_slot(0, 0, 0), w_slot(0, 0, 0), w_s.at[0, 3], w_r.at[0, 3], kv, tp_at(0, 1))
-    loads["dn"].wait()
-    send(w_slot(1, 0, 0), w_slot(1, 0, 0), w_s.at[1, 0], w_r.at[1, 0], kv, tp_at(1, 0))
-    send(w_slot(1, 0, 0), w_slot(1, 0, 0), w_s.at[1, 1], w_r.at[1, 1], kv, tp_at(3, 0))
-    send(w_slot(1, 0, 0), w_slot(1, 0, 0), w_s.at[1, 3], w_r.at[1, 3], kv, tp_at(0, 1))
 
     for name in ("ng", "q", "k", "v", "o", "ig", "fg", "fb", "stab", "nrm"):
         loads[name].wait()
@@ -161,7 +158,7 @@
         part = jnp.sum(mem[b] * qf[pl.ds(b, 1), :], axis=1, keepdims=True)
         return jnp.where(lane == b, part, acc)
 
-    read = lax.fori_loop(0, ROWS, read_memory, jnp.zeros((DK, DK), F32), unroll=4)
+    read = lax.fori_loop(0, ROWS, read_memory, jnp.zeros((DK, DK), F32), unroll=ROWS)
     memory_query = read.T[:ROWS, :]
     numer = keep * memory_query + (admit * key_query) * values
     cell = numer / jnp.maximum(jnp.abs(denom), 1.0)
@@ -170,6 +167,11 @@
     for k, (dy, dc) in enumerate(TPO):
         send(mx.at[:, lane_h], mx.at[:, lane_h], mix_s.at[k], mix_r.at[k], kv, tp_at(dy, dc))
 
+    loads["dn"].wait()
+    send(w_slot(1, 0, 0), w_slot(1, 0, 0), w_s.at[1, 0], w_r.at[1, 0], kv, tp_at(1, 0))
+    send(w_slot(1, 0, 0), w_slot(1, 0, 0), w_s.at[1, 1], w_r.at[1, 1], kv, tp_at(3, 0))
+    send(w_slot(1, 0, 0), w_slot(1, 0, 0), w_s.at[1, 3], w_r.at[1, 3], kv, tp_at(0, 1))
+
     nrmn_ref[...] = normalizer_new
     stabn_ref[...] = jnp.sum(
         jnp.where(diag, jnp.broadcast_to(stab_new, (ROWS, ROWS)), 0.0), axis=0, keepdims=True
@@ -185,7 +187,7 @@
         mem[b] = colrow[0, pl.ds(b, 1), :] * mem[b] + column * colrow[1, pl.ds(b, 1), :]
         return carry
 
-    lax.fori_loop(0, ROWS, write_memory, 0, unroll=4)
+    lax.fori_loop(0, ROWS, write_memory, 0, unroll=ROWS)
     store_mem = pltpu.make_async_copy(mem, memn_h, lsem.at[len(loads)])
     store_mem.start()
 
@@ -200,9 +202,9 @@
         seg[s] = secf[SUB * s : SUB * (s + 1), :].astype(BF16)
 
     pl.semaphore_wait(zready, ZN - 1)
-    own_seg = pltpu.make_async_copy(seg.at[t], xbuf.at[0, 0, t], az_r.at[0])
-    own_seg.start()
-    for dz in (4, 3, 5, 2, 6, 1, 7, 0):
+    home = ZPOS[0]
+    pltpu.make_async_copy(seg.at[t], xbuf.at[0, home, t], az_r.at[home]).start()
+    for dz in ZSEND:
         there = ZPOS[(-dz) % ZN]
         for dy, dc in TPO if dz == 0 else TPO + ((0, 0),):
             s = tp_at(dy, dc)
@@ -222,14 +224,13 @@
     relay(0, 1, 1, None)
     relay(1, 0, 3, None)
 
-    for g in range(GROUPS):
-        for p in (2 * g, 2 * g + 1):
-            await_bytes(xbuf.at[0, p], az_r.at[p])
-        pair = pl.ds(2 * g, 2)
+    for dz in ZSEND:
+        p = ZPOS[dz]
+        await_bytes(xbuf.at[0, p], az_r.at[p])
         for dx in range(1, XN):
             send(
-                xbuf.at[0, pair], xbuf.at[(-dx) % XN, pair],
-                xf_s.at[dx - 1, g], xf_r.at[(-dx) % XN - 1, g], zx(0, dx), t,
+                xbuf.at[0, p], xbuf.at[(-dx) % XN, p],
+                xf_s.at[dx - 1, p], xf_r.at[(-dx) % XN - 1, p], zx(0, dx), t,
             )
 
     relay(0, 2, 2, None)
@@ -243,7 +244,8 @@
 
     def mixer(g):
         for dx in range(1, XN):
-            await_bytes(xbuf.at[dx, pl.ds(2 * g, 2)], xf_r.at[dx - 1, g])
+            for p in (2 * g, 2 * g + 1):
+                await_bytes(xbuf.at[dx, p], xf_r.at[dx - 1, p])
         for i in range(2 * XN):
             dx, p = i // 2, 2 * g + i % 2
             block = xbuf[dx, p].astype(F32)
@@ -283,18 +285,17 @@
             dz = ZORD[p]
             there = ZPOS[(-dz) % ZN]
             if dz == 0:
-                pltpu.make_async_copy(zs.at[p, t], fin.at[0, t], fi_r.at[0]).start()
+                pltpu.make_async_copy(zs.at[p, t], fin.at[home, t], fi_r.at[home]).start()
             for dy, dc in TPO if dz == 0 else TPO + ((0, 0),):
                 s = tp_at(dy, dc)
                 remote(
                     zs.at[p, s], fin.at[there, t], fi_s.at[p], fi_r.at[there], zx(dz, 0), s
                 ).start()
 
-    mixer(0)
-    for g in range(1, GROUPS):
+    for g in range(GROUPS):
         mixer(g)
-        sum_x(g - 1)
-    sum_x(GROUPS - 1)
+    for g in range(GROUPS):
+        sum_x(g)
 
     total = jnp.zeros((TN, SUB, DB), F32)
     for p in range(ZN):
@@ -307,7 +308,7 @@
     for src, sem in pending:
         await_bytes(src, sem)
     for p in range(ZN):
-        count = TN - 1 if p == 0 else TN
+        count = TN - 1 if p == home else TN
         await_bytes(seg.at[pl.ds(0, count)], az_s.at[p])
         await_bytes(zs.at[p, pl.ds(0, count)], fi_s.at[p])
     store_mem.wait()
@@ -378,7 +379,7 @@
             dma((7,)), dma((7,)),
             dma((2, 7)), dma((2, 7)),
             dma((ZN,)), dma((ZN,)),
-            dma((XN - 1, GROUPS)), dma((XN - 1, GROUPS)),
+            dma((XN - 1, ZN)), dma((XN - 1, ZN)),
             dma((XN - 1, GROUPS)), dma((XN - 1, GROUPS)),
             dma((ZN,)), dma((ZN,)),
             pltpu.SemaphoreType.REGULAR,

time: 51.7 us -> 47.6 us (0.921)
  Pallas kernels: 50.9 us -> 46.8 us
    pallas_call x1, Pallas kernels: 49.6 us -> 45.5 us  [per_device(): pl.pallas_call(kernel, out_shape=outs, in_specs=[hbm] * 17, out_specs=(vm...]
where the time goes in v3:
time: 47.6 us; the launch traced here: 47.5 us
  Pallas kernels  46.8 us (98%)
  between operations  0.65 us (1%)
    pallas_call x1, Pallas kernels, per_device(): pl.pallas_call(kernel, out_shape=outs, in_specs=[hbm] * 17, out_specs=(vm...  45.5 us
    pallas_call x1, Pallas kernels, per_device(): pl.pallas_call(write_out, out_shape=outs, in_specs=[anywhere] * 4, out_sp...  1.37 us

profile of v3, /device:TPU:1, one launch (start us, length us, event | category | flops | bytes accessed | tf_op | source)
XLA Modules:
  0.0 47.5 jit_solution(1299274901123740082)
XLA Ops:
  0.6 45.5 %layer.1 = (bf16[32,256]{1,0:T(8,128)(2,1)S(1)}, f32[32,128,128]{2,1,0:T(8,128)S(1)}, f32[32,128]{1,0:T(8,128)S(1)}, f32[1,32]{1,0:T(1,128)S(1)}) custom-call(bf16[32,256]{1,0:T(8,128)(2,1)} %tok_h.1, f32[32,128,128]{2,1,0:T(8,128)} %bitcast.16, f32[32,128]{1,0:T(8,128)} %bitcast.19, f32[1,32]{1,0:T(1,128)} %bitcast.22, f32[1,2048]{1,0:T(1,128)} %bitcast.20, ...), custom_call_target="tpu_custom_call" | custom-call | tf_op jit(solution)/shard_map/layer/pallas_call | solution.py:340
  46.1 1.4 %write_out.1 = (bf16[32,256]{1,0:T(8,128)(2,1)}, f32[32,128,128]{2,1,0:T(8,128)}, f32[32,128]{1,0:T(8,128)}, f32[1,32]{1,0:T(1,128)}) custom-call(bf16[32,256]{1,0:T(8,128)(2,1)S(1)} %get-tuple-element.12.refs_0_, f32[32,128,128]{2,1,0:T(8,128)S(1)} %get-tuple-element.13.refs_1_, f32[32,128]{1,0:T(8,128)S(1)} %get-tuple-element.14.refs_2_, ...), custom_call_target="tpu_custom_call" | custom-call | tf_op jit(solution)/shard_map/write_out/pallas_call | solution.py:412

commit v4 on v3

--- a/solution.py
+++ b/solution.py
@@ -16,11 +16,16 @@
 DB = D // TN
 SUB = ROWS // TN
 FB = 256
-ZORD = (7, 2, 6, 3, 5, 4, 1, 0)
+ZORD = (0, 1, 7, 2, 6, 3, 5, 4)
 ZSEND = (0, 1, 7, 2, 6, 3, 5, 4)
+DIRECT_IN = ()
+DIRECT_OUT = (4,)
+ORDER = (
+    "f0", "f1", "f7", "f2", "f6", "r0", "r1", "f3", "f5", "f4", "r2", "r3", "w",
+    "m0", "m72", "m63", "m54", "m1", "s0", "s7", "s2", "s6", "s3", "s5", "s1",
+)
 ZPOS = tuple(ZORD.index(o) for o in range(ZN))
 TPO = ((2, 0), (2, 1), (1, 0), (1, 1), (3, 0), (3, 1), (0, 1))
-GROUPS = ZN // 2
 F32 = jnp.float32
 BF16 = jnp.bfloat16
 MESH = pl.DeviceIdType.MESH
@@ -47,7 +52,7 @@
     tk, mem, nrm, stab, ng, qkvo, ig, fg, fb, mg, pw, gains, upb, dnb,
     nb, qf, colrow, colmat, mx, secf, seg, xbuf, xs, os, rsx_s, rsx_r, own, zs, fin, of,
     lsem, tok_s, tok_r, gain_s, gain_r, mix_s, mix_r, w_s, w_r, az_s, az_r, xf_s, xf_r, rx_s, rx_r, fi_s, fi_r,
-    zready,
+    zready, xready,
 ):
     kv = lax.axis_index("kv")
     t = lax.axis_index("tp")
@@ -93,16 +98,19 @@
     load("mg", mg_h, mg)
     load("pw", pw_h, pw)
 
+    def tell(sem, kv_to, tp_to):
+        pl.semaphore_signal(sem, inc=1, device_id={"kv": kv_to, "tp": tp_to}, device_id_type=MESH)
+
     barrier = pltpu.get_barrier_semaphore()
     for dy, dc in TPO:
-        pl.semaphore_signal(barrier, inc=1, device_id={"kv": kv, "tp": tp_at(dy, dc)}, device_id_type=MESH)
-    for dx in range(1, XN):
-        pl.semaphore_signal(barrier, inc=1, device_id={"kv": zx(0, dx), "tp": t}, device_id_type=MESH)
-    for dz in range(1, ZN):
-        pl.semaphore_signal(barrier, inc=1, device_id={"kv": zx(dz, 0), "tp": t}, device_id_type=MESH)
-    pl.semaphore_wait(barrier, 7 + (XN - 1) + (ZN - 1))
-    for dz in range(1, ZN):
-        pl.semaphore_signal(zready, inc=1, device_id={"kv": zx(dz, 0), "tp": t}, device_id_type=MESH)
+        tell(barrier, kv, tp_at(dy, dc))
+    for step in (1, -1):
+        tell(barrier, zx(0, step), t)
+        tell(barrier, zx(step, 0), t)
+    pl.semaphore_wait(barrier, 7 + 4)
+    for step in (1, -1):
+        tell(xready.at[0], zx(0, step), t)
+        tell(zready.at[0], zx(step, 0), t)
 
     loads["tok"].wait()
     for k, (dy, dc) in enumerate(TPO):
@@ -113,18 +121,32 @@
 
     def w_slot(m, dy, dc):
         s = tp_at(dy, dc)
-        return upb.at[pl.ds(pl.multiple_of(s * DB, DB), DB)] if m == 0 else dnb.at[s]
+        if m < 2:
+            return upb.at[pl.ds(pl.multiple_of(s * DB + DB // 2 * m, DB // 2), DB // 2)]
+        return dnb.at[s, pl.ds(FB // 2 * (m - 2), FB // 2)]
+
+    def send_weights(m):
+        slot = w_slot(m, 0, 0)
+        for k, (dy, dc) in ((0, (1, 0)), (1, (3, 0)), (3, (0, 1))):
+            send(slot, slot, w_s.at[m, k], w_r.at[m, k], kv, tp_at(dy, dc))
 
     loads["up"].wait()
-    send(w_slot(0, 0, 0), w_slot(0, 0, 0), w_s.at[0, 0], w_r.at[0, 0], kv, tp_at(1, 0))
-    send(w_slot(0, 0, 0), w_slot(0, 0, 0), w_s.at[0, 1], w_r.at[0, 1], kv, tp_at(3, 0))
-    send(w_slot(0, 0, 0), w_slot(0, 0, 0), w_s.at[0, 3], w_r.at[0, 3], kv, tp_at(0, 1))
+    send_weights(0)
+    send_weights(1)
+
+    pl.semaphore_wait(xready.at[0], 2)
+    pl.semaphore_wait(zready.at[0], 2)
+    for step in (2, -2):
+        tell(zready.at[1], zx(step, 0), t)
 
     for name in ("ng", "q", "k", "v", "o", "ig", "fg", "fb", "stab", "nrm"):
         loads[name].wait()
     for k, (dy, dc) in enumerate(TPO):
         s = tp_at(-dy, -dc)
         await_bytes(tk.at[:, pl.ds(pl.multiple_of(s * DB, DB), DB)], tok_r.at[k])
+    pl.semaphore_wait(zready.at[1], 2)
+    for step in (3, -3, 4):
+        tell(zready.at[2], zx(step, 0), t)
     rows = tk[...].astype(F32)
     scale_one = lax.rsqrt(jnp.sum(rows * rows, axis=-1, keepdims=True) * (1.0 / D) + EPS)
     nb[...] = (rows * scale_one * ng[...]).astype(BF16)
@@ -168,9 +190,11 @@
         send(mx.at[:, lane_h], mx.at[:, lane_h], mix_s.at[k], mix_r.at[k], kv, tp_at(dy, dc))
 
     loads["dn"].wait()
-    send(w_slot(1, 0, 0), w_slot(1, 0, 0), w_s.at[1, 0], w_r.at[1, 0], kv, tp_at(1, 0))
-    send(w_slot(1, 0, 0), w_slot(1, 0, 0), w_s.at[1, 1], w_r.at[1, 1], kv, tp_at(3, 0))
-    send(w_slot(1, 0, 0), w_slot(1, 0, 0), w_s.at[1, 3], w_r.at[1, 3], kv, tp_at(0, 1))
+    send_weights(2)
+    send_weights(3)
+    pl.semaphore_wait(zready.at[2], 3)
+    for dx in range(1, XN):
+        tell(xready.at[1], zx(0, dx), t)
 
     nrmn_ref[...] = normalizer_new
     stabn_ref[...] = jnp.sum(
@@ -190,6 +214,13 @@
     lax.fori_loop(0, ROWS, write_memory, 0, unroll=ROWS)
     store_mem = pltpu.make_async_copy(mem, memn_h, lsem.at[len(loads)])
     store_mem.start()
+
+    def relay(m, k, dy, forward):
+        slot = w_slot(m, dy, 0)
+        await_bytes(slot, w_r.at[m, k])
+        if forward is not None:
+            send(slot, slot, w_s.at[m, 2], w_r.at[m, 2], kv, tp_at(forward, 0))
+        send(slot, slot, w_s.at[m, 4 + k], w_r.at[m, 4 + k], kv, tp_at(0, 1))
 
     loads["pw"].wait()
     for k, (dy, dc) in enumerate(TPO):
@@ -201,106 +232,117 @@
     for s in range(TN):
         seg[s] = secf[SUB * s : SUB * (s + 1), :].astype(BF16)
 
-    pl.semaphore_wait(zready, ZN - 1)
-    home = ZPOS[0]
-    pltpu.make_async_copy(seg.at[t], xbuf.at[0, home, t], az_r.at[home]).start()
+    def scatter(dz, dx, src, dst, ssem, rsem):
+        there = ZPOS[(-dz) % ZN]
+        slot = (-dx) % XN
+        for dy, dc in TPO + ((0, 0),):
+            s = tp_at(dy, dc)
+            if dz == 0 and dx == 0 and (dy, dc) == (0, 0):
+                pltpu.make_async_copy(src.at[s], dst.at[slot, there, t], rsem.at[slot, there]).start()
+            else:
+                remote(
+                    src.at[s], dst.at[slot, there, t], ssem.at[dx, ZPOS[dz]], rsem.at[slot, there], zx(dz, dx), s
+                ).start()
+
+    def targets(dz, direct):
+        return range(XN) if dz in direct else (0,)
+
+    pl.semaphore_wait(xready.at[1], XN - 1)
     for dz in ZSEND:
-        there = ZPOS[(-dz) % ZN]
-        for dy, dc in TPO if dz == 0 else TPO + ((0, 0),):
-            s = tp_at(dy, dc)
-            remote(
-                seg.at[s], xbuf.at[0, there, t], az_s.at[ZPOS[dz]], az_r.at[there], zx(dz, 0), s
-            ).start()
-
-    def relay(m, k, dy, forward):
-        slot = w_slot(m, dy, 0)
-        await_bytes(slot, w_r.at[m, k])
-        if forward is not None:
-            send(slot, slot, w_s.at[m, 2], w_r.at[m, 2], kv, tp_at(forward, 0))
-        send(slot, slot, w_s.at[m, 4 + k], w_r.at[m, 4 + k], kv, tp_at(0, 1))
+        for dx in targets(dz, DIRECT_IN):
+            scatter(dz, dx, seg, xbuf, az_s, az_r)
 
     relay(0, 0, 3, 1)
     relay(1, 1, 1, 3)
     relay(0, 1, 1, None)
     relay(1, 0, 3, None)
-
-    for dz in ZSEND:
+    relay(2, 1, 1, 3)
+    relay(3, 0, 3, 1)
+    relay(2, 0, 3, None)
+    relay(3, 1, 1, None)
+
+    def forward(dz):
         p = ZPOS[dz]
-        await_bytes(xbuf.at[0, p], az_r.at[p])
+        await_bytes(xbuf.at[0, p], az_r.at[0, p])
         for dx in range(1, XN):
             send(
                 xbuf.at[0, p], xbuf.at[(-dx) % XN, p],
                 xf_s.at[dx - 1, p], xf_r.at[(-dx) % XN - 1, p], zx(0, dx), t,
             )
 
-    relay(0, 2, 2, None)
-    relay(1, 2, 2, None)
-    for k, (dy, dc) in enumerate(TPO):
-        s = tp_at(-dy, -dc)
-        await_bytes(gains.at[:, pl.ds(pl.multiple_of(s * DB, DB), DB)], gain_r.at[k])
-    for m in range(2):
-        for k, dy in ((3, 0), (4, 3), (5, 1), (6, 2)):
-            await_bytes(w_slot(m, dy, 1), w_r.at[m, k])
-
-    def mixer(g):
-        for dx in range(1, XN):
-            for p in (2 * g, 2 * g + 1):
+    def rest_of_weights():
+        for k, (dy, dc) in enumerate(TPO):
+            s = tp_at(-dy, -dc)
+            await_bytes(gains.at[:, pl.ds(pl.multiple_of(s * DB, DB), DB)], gain_r.at[k])
+        for m in range(4):
+            for k, dy in ((3, 0), (4, 3), (5, 1), (6, 2)):
+                await_bytes(w_slot(m, dy, 1), w_r.at[m, k])
+
+    def mixer(group):
+        blocks = [(dx, ZPOS[dz]) for dx in range(XN) for dz in group]
+        count = SUB * len(blocks)
+        for dx, p in blocks:
+            if ZORD[p] in DIRECT_IN:
+                await_bytes(xbuf.at[dx, p], az_r.at[dx, p])
+            elif dx > 0:
                 await_bytes(xbuf.at[dx, p], xf_r.at[dx - 1, p])
-        for i in range(2 * XN):
-            dx, p = i // 2, 2 * g + i % 2
+        for i, (dx, p) in enumerate(blocks):
             block = xbuf[dx, p].astype(F32)
             for j in range(TN):
                 xs[SUB * i : SUB * (i + 1), DB * j : DB * (j + 1)] = block[j]
-        sec = xs[...]
+        sec = xs[:count, :]
         scale_two = lax.rsqrt(jnp.sum(sec * sec, axis=-1, keepdims=True) * (1.0 / D) + EPS)
         scaled = (sec * gains[...]).astype(BF16)
         preact = jnp.dot(scaled, upb[...], preferred_element_type=F32)
         hidden = jnp.square(jnp.maximum(preact * scale_two, 0.0)).astype(BF16)
         for j in range(TN):
-            os[:, DB * j : DB * (j + 1)] = jnp.dot(hidden, dnb[j], preferred_element_type=F32)
-        for i in range(2 * XN):
-            dx, p = i // 2, 2 * g + i % 2
+            os[:count, DB * j : DB * (j + 1)] = jnp.dot(hidden, dnb[j], preferred_element_type=F32)
+        for i, (dx, p) in enumerate(blocks):
             for j in range(TN):
                 block = os[SUB * i : SUB * (i + 1), DB * j : DB * (j + 1)]
-                if dx == 0:
+                if dx == 0 and ZORD[p] not in DIRECT_OUT:
                     own[p, j] = block
                 else:
-                    rsx_s[dx - 1, p, j] = block.astype(BF16)
-        pair = pl.ds(2 * g, 2)
+                    rsx_s[dx, p, j] = block.astype(BF16)
+        for dz in group:
+            p = ZPOS[dz]
+            if dz in DIRECT_OUT:
+                for dx in range(XN):
+                    scatter(dz, dx, rsx_s.at[dx, p], fin, fi_s, fi_r)
+            else:
+                for dx in range(1, XN):
+                    send(
+                        rsx_s.at[dx, p], rsx_r.at[(-dx) % XN - 1, p],
+                        rx_s.at[dx - 1, p], rx_r.at[(-dx) % XN - 1, p], zx(0, dx), t,
+                    )
+
+    def sum_x(p):
         for dx in range(1, XN):
-            send(
-                rsx_s.at[dx - 1, pair], rsx_r.at[(-dx) % XN - 1, pair],
-                rx_s.at[dx - 1, g], rx_r.at[(-dx) % XN - 1, g], zx(0, dx), t,
-            )
-
-    def sum_x(g):
-        pair = pl.ds(2 * g, 2)
+            await_bytes(rsx_r.at[dx - 1, p], rx_r.at[dx - 1, p])
+        total = own[p]
         for dx in range(1, XN):
-            await_bytes(rsx_r.at[dx - 1, pair], rx_r.at[dx - 1, g])
-        for p in (2 * g, 2 * g + 1):
-            total = own[p]
-            for dx in range(1, XN):
-                total += rsx_r[dx - 1, p].astype(F32)
-            zs[p] = total.astype(BF16)
-            dz = ZORD[p]
-            there = ZPOS[(-dz) % ZN]
-            if dz == 0:
-                pltpu.make_async_copy(zs.at[p, t], fin.at[home, t], fi_r.at[home]).start()
-            for dy, dc in TPO if dz == 0 else TPO + ((0, 0),):
-                s = tp_at(dy, dc)
-                remote(
-                    zs.at[p, s], fin.at[there, t], fi_s.at[p], fi_r.at[there], zx(dz, 0), s
-                ).start()
-
-    for g in range(GROUPS):
-        mixer(g)
-    for g in range(GROUPS):
-        sum_x(g)
+            total += rsx_r[dx - 1, p].astype(F32)
+        zs[p] = total.astype(BF16)
+        scatter(ZORD[p], 0, zs.at[p], fin, fi_s, fi_r)
+
+    for step in ORDER:
+        group = [int(digit) for digit in step[1:]]
+        if step == "w":
+            rest_of_weights()
+        elif step[0] == "r":
+            relay(group[0], 2, 2, None)
+        elif step[0] == "f":
+            forward(group[0])
+        elif step[0] == "m":
+            mixer(group)
+        else:
+            sum_x(ZPOS[group[0]])
 
     total = jnp.zeros((TN, SUB, DB), F32)
     for p in range(ZN):
-        await_bytes(fin.at[p], fi_r.at[p])
-        total += fin[p].astype(F32)
+        for dx in targets(ZORD[p], DIRECT_OUT):
+            await_bytes(fin.at[dx, p], fi_r.at[dx, p])
+            total += fin[dx, p].astype(F32)
     for s in range(TN):
         of[SUB * s : SUB * (s + 1), :] = total[s]
     out_ref[...] = (secf[...] + of[...]).astype(BF16)
@@ -308,15 +350,18 @@
     for src, sem in pending:
         await_bytes(src, sem)
     for p in range(ZN):
-        count = TN - 1 if p == home else TN
-        await_bytes(seg.at[pl.ds(0, count)], az_s.at[p])
-        await_bytes(zs.at[p, pl.ds(0, count)], fi_s.at[p])
+        for refs, direct in ((az_s, DIRECT_IN), (fi_s, DIRECT_OUT)):
+            for dx in targets(ZORD[p], direct):
+                count = TN - 1 if ZORD[p] == 0 and dx == 0 else TN
+                await_bytes(seg.at[pl.ds(0, count)], refs.at[dx, p])
     store_mem.wait()
 
 
 def write_out(*refs):
     ins, outs, sems = refs[:4], refs[4:8], refs[8]
-    copies = [pltpu.make_async_copy(src, dst, sems.at[k]) for k, (src, dst) in enumerate(zip(ins, outs))]
+    pairs = [(ins[k], outs[k]) for k in (0, 2, 3)]
+    pairs += [(ins[1].at[pl.ds(k, 4)], outs[1].at[pl.ds(k, 4)]) for k in range(0, ROWS, 4)]
+    copies = [pltpu.make_async_copy(src, dst, sems.at[k]) for k, (src, dst) in enumerate(pairs)]
     for copy in copies:
         copy.start()
     for copy in copies:
@@ -367,22 +412,23 @@
             pltpu.VMEM((XN, ZN, TN, SUB, DB), BF16),
             pltpu.VMEM((ROWS, D), F32),
             pltpu.VMEM((ROWS, D), F32),
-            pltpu.VMEM((XN - 1, ZN, TN, SUB, DB), BF16),
+            pltpu.VMEM((XN, ZN, TN, SUB, DB), BF16),
             pltpu.VMEM((XN - 1, ZN, TN, SUB, DB), BF16),
             pltpu.VMEM((ZN, TN, SUB, DB), F32),
             pltpu.VMEM((ZN, TN, SUB, DB), BF16),
-            pltpu.VMEM((ZN, TN, SUB, DB), BF16),
+            pltpu.VMEM((XN, ZN, TN, SUB, DB), BF16),
             pltpu.VMEM((ROWS, DB), F32),
             dma((18,)),
             dma((7,)), dma((7,)),
             dma((7,)), dma((7,)),
             dma((7,)), dma((7,)),
-            dma((2, 7)), dma((2, 7)),
-            dma((ZN,)), dma((ZN,)),
+            dma((4, 7)), dma((4, 7)),
+            dma((XN, ZN)), dma((XN, ZN)),
             dma((XN - 1, ZN)), dma((XN - 1, ZN)),
-            dma((XN - 1, GROUPS)), dma((XN - 1, GROUPS)),
-            dma((ZN,)), dma((ZN,)),
-            pltpu.SemaphoreType.REGULAR,
+            dma((XN - 1, ZN)), dma((XN - 1, ZN)),
+            dma((XN, ZN)), dma((XN, ZN)),
+            pltpu.SemaphoreType.REGULAR((3,)),
+            pltpu.SemaphoreType.REGULAR((2,)),
         ],
         compiler_params=pltpu.CompilerParams(
             collective_id=0, has_side_effects=True, vmem_limit_bytes=40 * 1024 * 1024
@@ -414,7 +460,7 @@
         out_shape=outs,
         in_specs=[anywhere] * 4,
         out_specs=(hbm,) * 4,
-        scratch_shapes=[dma((4,))],
+        scratch_shapes=[dma((11,))],
         compiler_params=pltpu.CompilerParams(vmem_limit_bytes=4 * 1024 * 1024),
         name="write_out",
     )(layer_out, memory_new, normalizer_new, stab_new)

time: 47.6 us -> 47.3 us (level)
  no operation moved by 1% of the time
where the time goes in v4:
time: 47.3 us; the launch traced here: 47.2 us
  Pallas kernels  46.6 us (99%)
  between operations  0.65 us (1%)
    pallas_call x1, Pallas kernels, per_device(): pl.pallas_call(kernel, out_shape=outs, in_specs=[hbm] * 17, out_specs=(vm...  45.2 us
    pallas_call x1, Pallas kernels, per_device(): pl.pallas_call(write_out, out_shape=outs, in_specs=[anywhere] * 4, out_sp...  1.42 us

profile of v4, /device:TPU:1, one launch (start us, length us, event | category | flops | bytes accessed | tf_op | source)
XLA Modules:
  0.0 47.2 jit_solution(2259678017280311337)
XLA Ops:
  0.6 45.2 %layer.1 = (bf16[32,256]{1,0:T(8,128)(2,1)S(1)}, f32[32,128,128]{2,1,0:T(8,128)S(1)}, f32[32,128]{1,0:T(8,128)S(1)}, f32[1,32]{1,0:T(1,128)S(1)}) custom-call(bf16[32,256]{1,0:T(8,128)(2,1)} %tok_h.1, f32[32,128,128]{2,1,0:T(8,128)} %bitcast.16, f32[32,128]{1,0:T(8,128)} %bitcast.19, f32[1,32]{1,0:T(1,128)} %bitcast.22, f32[1,2048]{1,0:T(1,128)} %bitcast.20, ...), custom_call_target="tpu_custom_call" | custom-call | tf_op jit(solution)/shard_map/layer/pallas_call | solution.py:385
  45.8 1.4 %write_out.1 = (bf16[32,256]{1,0:T(8,128)(2,1)}, f32[32,128,128]{2,1,0:T(8,128)}, f32[32,128]{1,0:T(8,128)}, f32[1,32]{1,0:T(1,128)}) custom-call(bf16[32,256]{1,0:T(8,128)(2,1)S(1)} %get-tuple-element.12.refs_0_, f32[32,128,128]{2,1,0:T(8,128)S(1)} %get-tuple-element.13.refs_1_, f32[32,128]{1,0:T(8,128)S(1)} %get-tuple-element.14.refs_2_, ...), custom_call_target="tpu_custom_call" | custom-call | tf_op jit(solution)/shard_map/write_out/pallas_call | solution.py:458

commit v5 on v4

--- a/solution.py
+++ b/solution.py
@@ -17,14 +17,16 @@
 SUB = ROWS // TN
 FB = 256
 ZORD = (0, 1, 7, 2, 6, 3, 5, 4)
-ZSEND = (0, 1, 7, 2, 6, 3, 5, 4)
-DIRECT_IN = ()
+ZSEND = (0, 2, 6, 3, 5, 4)
+NEXT = (1, 7)
+DIRECT_IN = (0,)
 DIRECT_OUT = (4,)
 ORDER = (
-    "f0", "f1", "f7", "f2", "f6", "r0", "r1", "f3", "f5", "f4", "r2", "r3", "w",
-    "m0", "m72", "m63", "m54", "m1", "s0", "s7", "s2", "s6", "s3", "s5", "s1",
+    "d", "f2", "f6", "r0", "r1", "f3", "f5", "r2", "r3", "f4", "w",
+    "m0", "m17", "m26", "m35", "m4", "z", "s2", "s6", "s3", "s5", "s0",
 )
 ZPOS = tuple(ZORD.index(o) for o in range(ZN))
+HOME = ZPOS[0]
 TPO = ((2, 0), (2, 1), (1, 0), (1, 1), (3, 0), (3, 1), (0, 1))
 F32 = jnp.float32
 BF16 = jnp.bfloat16
@@ -50,8 +52,8 @@
     tok_h, mem_h, nrm_h, stab_h, ng_h, qw_h, kw_h, vw_h, ow_h, ig_h, fg_h, fb_h, mg_h, pw_h, gain_h, up_h, dn_h,
     out_ref, memn_h, nrmn_ref, stabn_ref,
     tk, mem, nrm, stab, ng, qkvo, ig, fg, fb, mg, pw, gains, upb, dnb,
-    nb, qf, colrow, colmat, mx, secf, seg, xbuf, xs, os, rsx_s, rsx_r, own, zs, fin, of,
-    lsem, tok_s, tok_r, gain_s, gain_r, mix_s, mix_r, w_s, w_r, az_s, az_r, xf_s, xf_r, rx_s, rx_r, fi_s, fi_r,
+    qf, colrow, colmat, mx, secf, seg, xbuf, xs, os, rsx_s, rsx_r, own, own_row, rows_z, zs, fin, of,
+    lsem, tok_s, tok_r, gain_s, gain_r, mix_s, mix_r, w_s, w_r, az_s, az_r, xf_s, xf_r, rx_s, rx_r, fi_s, fi_r, gz_s, gz_r, hz_s, hz_r,
     zready, xready,
 ):
     kv = lax.axis_index("kv")
@@ -139,27 +141,44 @@
     for step in (2, -2):
         tell(zready.at[1], zx(step, 0), t)
 
+    def chip_slice(dy, width):
+        return pl.ds(pl.multiple_of(((y - dy) % YN) * 2 * width, 2 * width), 2 * width)
+
+    def await_chip(dy, recv):
+        for k, (other, dc) in enumerate(TPO):
+            if other == dy:
+                await_bytes(recv[0](tp_at(-dy, -dc)), recv[1].at[k])
+
     for name in ("ng", "q", "k", "v", "o", "ig", "fg", "fb", "stab", "nrm"):
         loads[name].wait()
-    for k, (dy, dc) in enumerate(TPO):
-        s = tp_at(-dy, -dc)
-        await_bytes(tk.at[:, pl.ds(pl.multiple_of(s * DB, DB), DB)], tok_r.at[k])
-    pl.semaphore_wait(zready.at[1], 2)
-    for step in (3, -3, 4):
-        tell(zready.at[2], zx(step, 0), t)
-    rows = tk[...].astype(F32)
-    scale_one = lax.rsqrt(jnp.sum(rows * rows, axis=-1, keepdims=True) * (1.0 / D) + EPS)
-    nb[...] = (rows * scale_one * ng[...]).astype(BF16)
-    proj4 = jnp.dot(nb[...], qkvo[...], preferred_element_type=F32).astype(BF16).astype(F32)
+    contract = (((1,), (1,)), ((), ()))
+    square_sum = jnp.zeros((ROWS, 1), F32)
+    proj4 = jnp.zeros((ROWS, 4 * DK), F32)
+    all_in = jnp.zeros((ROWS, TN), F32)
+    all_forget = jnp.zeros((ROWS, TN), F32)
+    for dy in (0, 1, 3, 2):
+        if dy == 1:
+            pl.semaphore_wait(zready.at[1], 2)
+            for step in (3, -3, 4):
+                tell(zready.at[2], zx(step, 0), t)
+        await_chip(dy, (lambda s: tk.at[:, pl.ds(pl.multiple_of(s * DB, DB), DB)], tok_r))
+        cols = chip_slice(dy, DB)
+        rows = tk[:, cols].astype(F32)
+        square_sum += jnp.sum(rows * rows, axis=-1, keepdims=True)
+        gained = (rows * ng[:, cols]).astype(BF16)
+        proj4 += jnp.dot(gained, qkvo[cols, :], preferred_element_type=F32)
+        all_in += lax.dot_general(gained, ig[:, cols], contract, preferred_element_type=F32)
+        all_forget += lax.dot_general(gained, fg[:, cols], contract, preferred_element_type=F32)
+    scale_one = lax.rsqrt(square_sum * (1.0 / D) + EPS)
+    proj4 = (proj4 * scale_one).astype(BF16).astype(F32)
     query = proj4[:, :DK]
     keys = proj4[:, DK : 2 * DK] * DK ** (-0.5)
     values = proj4[:, 2 * DK : 3 * DK]
     gate_out = proj4[:, 3 * DK :]
     qf[...] = query
 
-    contract = (((1,), (1,)), ((), ()))
-    all_in = lax.dot_general(nb[...], ig[...], contract, preferred_element_type=F32)
-    all_forget = lax.dot_general(nb[...], fg[...], contract, preferred_element_type=F32) + fb[...]
+    all_in = all_in * scale_one
+    all_forget = all_forget * scale_one + fb[...]
     head = lax.broadcasted_iota(jnp.int32, (ROWS, TN), 1) == t
     input_log = jnp.sum(jnp.where(head, all_in, 0.0), axis=1, keepdims=True)
     raw = jnp.sum(jnp.where(head, all_forget, 0.0), axis=1, keepdims=True)
@@ -192,10 +211,6 @@
     loads["dn"].wait()
     send_weights(2)
     send_weights(3)
-    pl.semaphore_wait(zready.at[2], 3)
-    for dx in range(1, XN):
-        tell(xready.at[1], zx(0, dx), t)
-
     nrmn_ref[...] = normalizer_new
     stabn_ref[...] = jnp.sum(
         jnp.where(diag, jnp.broadcast_to(stab_new, (ROWS, ROWS)), 0.0), axis=0, keepdims=True
@@ -215,6 +230,10 @@
     store_mem = pltpu.make_async_copy(mem, memn_h, lsem.at[len(loads)])
     store_mem.start()
 
+    pl.semaphore_wait(zready.at[2], 3)
+    for dx in range(1, XN):
+        tell(xready.at[1], zx(0, dx), t)
+
     def relay(m, k, dy, forward):
         slot = w_slot(m, dy, 0)
         await_bytes(slot, w_r.at[m, k])
@@ -223,10 +242,11 @@
         send(slot, slot, w_s.at[m, 4 + k], w_r.at[m, 4 + k], kv, tp_at(0, 1))
 
     loads["pw"].wait()
-    for k, (dy, dc) in enumerate(TPO):
-        s = tp_at(-dy, -dc)
-        await_bytes(mx.at[:, pl.ds(pl.multiple_of(s * DK, DK), DK)], mix_r.at[k])
-    projected = jnp.dot(mx[...], pw[...], preferred_element_type=F32)
+    projected = jnp.zeros((ROWS, DB), F32)
+    for dy in (0, 1, 3, 2):
+        await_chip(dy, (lambda s: mx.at[:, pl.ds(pl.multiple_of(s * DK, DK), DK)], mix_r))
+        cols = chip_slice(dy, DK)
+        projected += jnp.dot(mx[:, cols], pw[cols, :], preferred_element_type=F32)
     second = (tk[:, lane_t].astype(F32) + projected).astype(BF16).astype(F32)
     secf[...] = second
     for s in range(TN):
@@ -245,6 +265,8 @@
                 ).start()
 
     def targets(dz, direct):
+        if dz in NEXT:
+            return ()
         return range(XN) if dz in direct else (0,)
 
     pl.semaphore_wait(xready.at[1], XN - 1)
@@ -270,6 +292,13 @@
                 xf_s.at[dx - 1, p], xf_r.at[(-dx) % XN - 1, p], zx(0, dx), t,
             )
 
+    def spread_row():
+        for dx in range(XN):
+            await_bytes(xbuf.at[dx, HOME], az_r.at[dx, HOME])
+        for k, dz in enumerate(NEXT):
+            there = ZPOS[(-dz) % ZN]
+            send(xbuf.at[:, HOME], xbuf.at[:, there], gz_s.at[k], gz_r.at[there - 1], zx(dz, 0), t)
+
     def rest_of_weights():
         for k, (dy, dc) in enumerate(TPO):
             s = tp_at(-dy, -dc)
@@ -278,14 +307,23 @@
             for k, dy in ((3, 0), (4, 3), (5, 1), (6, 2)):
                 await_bytes(w_slot(m, dy, 1), w_r.at[m, k])
 
+    def send_along_x(p):
+        for dx in range(1, XN):
+            send(
+                rsx_s.at[dx, p], rsx_r.at[(-dx) % XN - 1, p],
+                rx_s.at[dx - 1, p], rx_r.at[(-dx) % XN - 1, p], zx(0, dx), t,
+            )
+
     def mixer(group):
         blocks = [(dx, ZPOS[dz]) for dx in range(XN) for dz in group]
         count = SUB * len(blocks)
-        for dx, p in blocks:
-            if ZORD[p] in DIRECT_IN:
-                await_bytes(xbuf.at[dx, p], az_r.at[dx, p])
-            elif dx > 0:
-                await_bytes(xbuf.at[dx, p], xf_r.at[dx - 1, p])
+        for dz in group:
+            p = ZPOS[dz]
+            if dz in NEXT:
+                await_bytes(xbuf.at[:, p], gz_r.at[p - 1])
+            elif dz != 0:
+                for dx in range(1, XN):
+                    await_bytes(xbuf.at[dx, p], xf_r.at[dx - 1, p])
         for i, (dx, p) in enumerate(blocks):
             block = xbuf[dx, p].astype(F32)
             for j in range(TN):
@@ -300,7 +338,9 @@
         for i, (dx, p) in enumerate(blocks):
             for j in range(TN):
                 block = os[SUB * i : SUB * (i + 1), DB * j : DB * (j + 1)]
-                if dx == 0 and ZORD[p] not in DIRECT_OUT:
+                if p == HOME:
+                    own_row[dx, j] = block
+                elif dx == 0 and ZORD[p] not in DIRECT_OUT + NEXT:
                     own[p, j] = block
                 else:
                     rsx_s[dx, p, j] = block.astype(BF16)
@@ -309,12 +349,22 @@
             if dz in DIRECT_OUT:
                 for dx in range(XN):
                     scatter(dz, dx, rsx_s.at[dx, p], fin, fi_s, fi_r)
+            elif dz in NEXT:
+                there = ZPOS[(-dz) % ZN] - 1
+                send(rsx_s.at[:, p], rows_z.at[there], hz_s.at[p - 1], hz_r.at[there], zx(dz, 0), t)
+            elif dz != 0:
+                send_along_x(p)
+
+    def sum_z():
+        for k in range(2):
+            await_bytes(rows_z.at[k], hz_r.at[k])
+        for dx in range(XN):
+            total = own_row[dx] + rows_z[0, dx].astype(F32) + rows_z[1, dx].astype(F32)
+            if dx == 0:
+                own[HOME] = total
             else:
-                for dx in range(1, XN):
-                    send(
-                        rsx_s.at[dx, p], rsx_r.at[(-dx) % XN - 1, p],
-                        rx_s.at[dx - 1, p], rx_r.at[(-dx) % XN - 1, p], zx(0, dx), t,
-                    )
+                rsx_s[dx, HOME] = total.astype(BF16)
+        send_along_x(HOME)
 
     def sum_x(p):
         for dx in range(1, XN):
@@ -329,6 +379,10 @@
         group = [int(digit) for digit in step[1:]]
         if step == "w":
             rest_of_weights()
+        elif step == "d":
+            spread_row()
+        elif step == "z":
+            sum_z()
         elif step[0] == "r":
             relay(group[0], 2, 2, None)
         elif step[0] == "f":
@@ -402,7 +456,6 @@
             pltpu.VMEM((1, D), F32),
             pltpu.VMEM((D, FB), BF16),
             pltpu.VMEM((TN, FB, DB), BF16),
-            pltpu.VMEM((ROWS, D), BF16),
             pltpu.VMEM((ROWS, DK), F32),
             pltpu.VMEM((2, ROWS, DK), F32),
             pltpu.VMEM((DK, DK), F32),
@@ -415,6 +468,8 @@
             pltpu.VMEM((XN, ZN, TN, SUB, DB), BF16),
             pltpu.VMEM((XN - 1, ZN, TN, SUB, DB), BF16),
             pltpu.VMEM((ZN, TN, SUB, DB), F32),
+            pltpu.VMEM((XN, TN, SUB, DB), F32),
+            pltpu.VMEM((2, XN, TN, SUB, DB), BF16),
             pltpu.VMEM((ZN, TN, SUB, DB), BF16),
             pltpu.VMEM((XN, ZN, TN, SUB, DB), BF16),
             pltpu.VMEM((ROWS, DB), F32),
@@ -427,6 +482,8 @@
             dma((XN - 1, ZN)), dma((XN - 1, ZN)),
             dma((XN - 1, ZN)), dma((XN - 1, ZN)),
             dma((XN, ZN)), dma((XN, ZN)),
+            dma((2,)), dma((2,)),
+            dma((2,)), dma((2,)),
             pltpu.SemaphoreType.REGULAR((3,)),
             pltpu.SemaphoreType.REGULAR((2,)),
         ],

time: 47.3 us -> 45.7 us (0.966)
  Pallas kernels: 46.6 us -> 45 us
    pallas_call x1, Pallas kernels: 45.2 us -> 43.6 us  [per_device(): pl.pallas_call(kernel, out_shape=outs, in_specs=[hbm] * 17, out_specs=(vm...]
where the time goes in v5:
time: 45.7 us; the launch traced here: 45.6 us
  Pallas kernels  45 us (98%)
  between operations  0.65 us (1%)
    pallas_call x1, Pallas kernels, per_device(): pl.pallas_call(kernel, out_shape=outs, in_specs=[hbm] * 17, out_specs=(vm...  43.6 us
    pallas_call x1, Pallas kernels, per_device(): pl.pallas_call(write_out, out_shape=outs, in_specs=[anywhere] * 4, out_sp...  1.42 us

profile of v5, /device:TPU:1, one launch (start us, length us, event | category | flops | bytes accessed | tf_op | source)
XLA Modules:
  0.0 45.6 jit_solution(2817014855706380021)
XLA Ops:
  0.6 43.6 %layer.1 = (bf16[32,256]{1,0:T(8,128)(2,1)S(1)}, f32[32,128,128]{2,1,0:T(8,128)S(1)}, f32[32,128]{1,0:T(8,128)S(1)}, f32[1,32]{1,0:T(1,128)S(1)}) custom-call(bf16[32,256]{1,0:T(8,128)(2,1)} %tok_h.1, f32[32,128,128]{2,1,0:T(8,128)} %bitcast.16, f32[32,128]{1,0:T(8,128)} %bitcast.19, f32[1,32]{1,0:T(1,128)} %bitcast.22, f32[1,2048]{1,0:T(1,128)} %bitcast.20, ...), custom_call_target="tpu_custom_call" | custom-call | tf_op jit(solution)/shard_map/layer/pallas_call | solution.py:439
  44.2 1.4 %write_out.1 = (bf16[32,256]{1,0:T(8,128)(2,1)}, f32[32,128,128]{2,1,0:T(8,128)}, f32[32,128]{1,0:T(8,128)}, f32[1,32]{1,0:T(1,128)}) custom-call(bf16[32,256]{1,0:T(8,128)(2,1)S(1)} %get-tuple-element.12.refs_0_, f32[32,128,128]{2,1,0:T(8,128)S(1)} %get-tuple-element.13.refs_1_, f32[32,128]{1,0:T(8,128)S(1)} %get-tuple-element.14.refs_2_, ...), custom_call_target="tpu_custom_call" | custom-call | tf_op jit(solution)/shard_map/write_out/pallas_call | solution.py:515

commit v6 on v5

--- a/solution.py
+++ b/solution.py
@@ -17,13 +17,12 @@
 SUB = ROWS // TN
 FB = 256
 ZORD = (0, 1, 7, 2, 6, 3, 5, 4)
-ZSEND = (0, 2, 6, 3, 5, 4)
+ZSEND = (2, 6, 3, 5, 0, 4)
 NEXT = (1, 7)
 DIRECT_IN = (0,)
 DIRECT_OUT = (4,)
 ORDER = (
-    "d", "f2", "f6", "r0", "r1", "f3", "f5", "r2", "r3", "f4", "w",
-    "m0", "m17", "m26", "m35", "m4", "z", "s2", "s6", "s3", "s5", "s0",
+    "d", "f2", "f6", "r0", "r1", "f3", "f5", "r2", "r3", "f4", "w", "m0", "m17", "m26", "m35", "m4", "z", "s2", "s6", "s3", "s5", "s0",
 )
 ZPOS = tuple(ZORD.index(o) for o in range(ZN))
 HOME = ZPOS[0]
@@ -267,7 +266,7 @@
     def targets(dz, direct):
         if dz in NEXT:
             return ()
-        return range(XN) if dz in direct else (0,)
+        return (2, 1, 3, 0) if dz in direct else (0,)
 
     pl.semaphore_wait(xready.at[1], XN - 1)
     for dz in ZSEND:
@@ -286,7 +285,7 @@
     def forward(dz):
         p = ZPOS[dz]
         await_bytes(xbuf.at[0, p], az_r.at[0, p])
-        for dx in range(1, XN):
+        for dx in (2, 1, 3):
             send(
                 xbuf.at[0, p], xbuf.at[(-dx) % XN, p],
                 xf_s.at[dx - 1, p], xf_r.at[(-dx) % XN - 1, p], zx(0, dx), t,
@@ -308,7 +307,7 @@
                 await_bytes(w_slot(m, dy, 1), w_r.at[m, k])
 
     def send_along_x(p):
-        for dx in range(1, XN):
+        for dx in (2, 1, 3):
             send(
                 rsx_s.at[dx, p], rsx_r.at[(-dx) % XN - 1, p],
                 rx_s.at[dx - 1, p], rx_r.at[(-dx) % XN - 1, p], zx(0, dx), t,
@@ -321,7 +320,11 @@
             p = ZPOS[dz]
             if dz in NEXT:
                 await_bytes(xbuf.at[:, p], gz_r.at[p - 1])
-            elif dz != 0:
+            elif dz in DIRECT_IN:
+                if dz != 0:
+                    for dx in range(XN):
+                        await_bytes(xbuf.at[dx, p], az_r.at[dx, p])
+            else:
                 for dx in range(1, XN):
                     await_bytes(xbuf.at[dx, p], xf_r.at[dx - 1, p])
         for i, (dx, p) in enumerate(blocks):
@@ -347,7 +350,7 @@
         for dz in group:
             p = ZPOS[dz]
             if dz in DIRECT_OUT:
-                for dx in range(XN):
+                for dx in (2, 1, 3, 0):
                     scatter(dz, dx, rsx_s.at[dx, p], fin, fi_s, fi_r)
             elif dz in NEXT:
                 there = ZPOS[(-dz) % ZN] - 1
@@ -392,6 +395,13 @@
         else:
             sum_x(ZPOS[group[0]])
 
+    for src, sem in pending:
+        await_bytes(src, sem)
+    for p in range(ZN):
+        for dx in targets(ZORD[p], DIRECT_IN):
+            count = TN - 1 if ZORD[p] == 0 and dx == 0 else TN
+            await_bytes(seg.at[pl.ds(0, count)], az_s.at[dx, p])
+
     total = jnp.zeros((TN, SUB, DB), F32)
     for p in range(ZN):
         for dx in targets(ZORD[p], DIRECT_OUT):
@@ -401,21 +411,16 @@
         of[SUB * s : SUB * (s + 1), :] = total[s]
     out_ref[...] = (secf[...] + of[...]).astype(BF16)
 
-    for src, sem in pending:
-        await_bytes(src, sem)
     for p in range(ZN):
-        for refs, direct in ((az_s, DIRECT_IN), (fi_s, DIRECT_OUT)):
-            for dx in targets(ZORD[p], direct):
-                count = TN - 1 if ZORD[p] == 0 and dx == 0 else TN
-                await_bytes(seg.at[pl.ds(0, count)], refs.at[dx, p])
+        for dx in targets(ZORD[p], DIRECT_OUT):
+            count = TN - 1 if ZORD[p] == 0 and dx == 0 else TN
+            await_bytes(seg.at[pl.ds(0, count)], fi_s.at[dx, p])
     store_mem.wait()
 
 
 def write_out(*refs):
     ins, outs, sems = refs[:4], refs[4:8], refs[8]
-    pairs = [(ins[k], outs[k]) for k in (0, 2, 3)]
-    pairs += [(ins[1].at[pl.ds(k, 4)], outs[1].at[pl.ds(k, 4)]) for k in range(0, ROWS, 4)]
-    copies = [pltpu.make_async_copy(src, dst, sems.at[k]) for k, (src, dst) in enumerate(pairs)]
+    copies = [pltpu.make_async_copy(ins[k], outs[k], sems.at[k]) for k in (1, 0, 2, 3)]
     for copy in copies:
         copy.start()
     for copy in copies:
@@ -517,7 +522,7 @@
         out_shape=outs,
         in_specs=[anywhere] * 4,
         out_specs=(hbm,) * 4,
-        scratch_shapes=[dma((11,))],
+        scratch_shapes=[dma((4,))],
         compiler_params=pltpu.CompilerParams(vmem_limit_bytes=4 * 1024 * 1024),
         name="write_out",
     )(layer_out, memory_new, normalizer_new, stab_new)

time: 45.7 us -> 45 us (0.985)
  Pallas kernels: 45 us -> 44.2 us
    pallas_call x1, Pallas kernels: 43.6 us -> 42.9 us  [per_device(): pl.pallas_call(kernel, out_shape=outs, in_specs=[hbm] * 17, out_specs=(vm...]
where the time goes in v6:
time: 45 us; the launch traced here: 44.9 us
  Pallas kernels  44.2 us (98%)
  between operations  0.65 us (1%)
    pallas_call x1, Pallas kernels, per_device(): pl.pallas_call(kernel, out_shape=outs, in_specs=[hbm] * 17, out_specs=(vm...  42.9 us
    pallas_call x1, Pallas kernels, per_device(): pl.pallas_call(write_out, out_shape=outs, in_specs=[anywhere] * 4, out_sp...  1.36 us

profile of v6, /device:TPU:1, one launch (start us, length us, event | category | flops | bytes accessed | tf_op | source)
XLA Modules:
  0.0 44.9 jit_solution(15205228297385479111)
XLA Ops:
  0.6 42.9 %layer.1 = (bf16[32,256]{1,0:T(8,128)(2,1)S(1)}, f32[32,128,128]{2,1,0:T(8,128)S(1)}, f32[32,128]{1,0:T(8,128)S(1)}, f32[1,32]{1,0:T(1,128)S(1)}) custom-call(bf16[32,256]{1,0:T(8,128)(2,1)} %tok_h.1, f32[32,128,128]{2,1,0:T(8,128)} %bitcast.16, f32[32,128]{1,0:T(8,128)} %bitcast.19, f32[1,32]{1,0:T(1,128)} %bitcast.22, f32[1,2048]{1,0:T(1,128)} %bitcast.20, ...), custom_call_target="tpu_custom_call" | custom-call | tf_op jit(solution)/shard_map/layer/pallas_call | solution.py:444
  43.5 1.4 %write_out.1 = (bf16[32,256]{1,0:T(8,128)(2,1)}, f32[32,128,128]{2,1,0:T(8,128)}, f32[32,128]{1,0:T(8,128)}, f32[1,32]{1,0:T(1,128)}) custom-call(bf16[32,256]{1,0:T(8,128)(2,1)S(1)} %get-tuple-element.12.refs_0_, f32[32,128,128]{2,1,0:T(8,128)S(1)} %get-tuple-element.13.refs_1_, f32[32,128]{1,0:T(8,128)S(1)} %get-tuple-element.14.refs_2_, ...), custom_call_target="tpu_custom_call" | custom-call | tf_op jit(solution)/shard_map/write_out/pallas_call | solution.py:520

commit v7 on v6

--- a/solution.py
+++ b/solution.py
@@ -22,7 +22,7 @@
 DIRECT_IN = (0,)
 DIRECT_OUT = (4,)
 ORDER = (
-    "d", "f2", "f6", "r0", "r1", "f3", "f5", "r2", "r3", "f4", "w", "m0", "m17", "m26", "m35", "m4", "z", "s2", "s6", "s3", "s5", "s0",
+    "d", "f2", "f6", "r0", "r1", "f3", "f5", "r2", "r3", "f4", "w", "m17", "m26", "m35", "m4", "m0", "z", "s2", "s6", "s3", "s5", "s0",
 )
 ZPOS = tuple(ZORD.index(o) for o in range(ZN))
 HOME = ZPOS[0]
@@ -198,7 +198,17 @@
         part = jnp.sum(mem[b] * qf[pl.ds(b, 1), :], axis=1, keepdims=True)
         return jnp.where(lane == b, part, acc)
 
-    read = lax.fori_loop(0, ROWS, read_memory, jnp.zeros((DK, DK), F32), unroll=ROWS)
+    ones = jnp.ones((DK, DK), BF16)
+    read = jnp.zeros((DK, DK), F32)
+    for first in range(0, ROWS // 2, 4):
+        product = jnp.concatenate([mem[b] * qf[b : b + 1, :] for b in range(first, first + 4)], axis=0)
+        high = product.astype(BF16)
+        low = (product - high.astype(F32)).astype(BF16)
+        sums = jnp.dot(high, ones, preferred_element_type=F32) + jnp.dot(low, ones, preferred_element_type=F32)
+        for k in range(4):
+            read = jnp.where(lane == first + k, sums[DK * k : DK * (k + 1), :], read)
+        for b in range(ROWS // 2 + first, ROWS // 2 + first + 4):
+            read = read_memory(b, read)
     memory_query = read.T[:ROWS, :]
     numer = keep * memory_query + (admit * key_query) * values
     cell = numer / jnp.maximum(jnp.abs(denom), 1.0)

time: 45 us -> 44.6 us (level)
  no operation moved by 1% of the time
where the time goes in v7:
time: 44.6 us; the launch traced here: 44.5 us
  Pallas kernels  43.9 us (98%)
  between operations  0.65 us (1%)
    pallas_call x1, Pallas kernels, per_device(): pl.pallas_call(kernel, out_shape=outs, in_specs=[hbm] * 17, out_specs=(vm...  42.5 us
    pallas_call x1, Pallas kernels, per_device(): pl.pallas_call(write_out, out_shape=outs, in_specs=[anywhere] * 4, out_sp...  1.36 us

profile of v7, /device:TPU:1, one launch (start us, length us, event | category | flops | bytes accessed | tf_op | source)
XLA Modules:
  0.0 44.5 jit_solution(16066827077489432507)
XLA Ops:
  0.6 42.5 %layer.1 = (bf16[32,256]{1,0:T(8,128)(2,1)S(1)}, f32[32,128,128]{2,1,0:T(8,128)S(1)}, f32[32,128]{1,0:T(8,128)S(1)}, f32[1,32]{1,0:T(1,128)S(1)}) custom-call(bf16[32,256]{1,0:T(8,128)(2,1)} %tok_h.1, f32[32,128,128]{2,1,0:T(8,128)} %bitcast.16, f32[32,128]{1,0:T(8,128)} %bitcast.19, f32[1,32]{1,0:T(1,128)} %bitcast.22, f32[1,2048]{1,0:T(1,128)} %bitcast.20, ...), custom_call_target="tpu_custom_call" | custom-call | tf_op jit(solution)/shard_map/layer/pallas_call | solution.py:454
  43.1 1.4 %write_out.1 = (bf16[32,256]{1,0:T(8,128)(2,1)}, f32[32,128,128]{2,1,0:T(8,128)}, f32[32,128]{1,0:T(8,128)}, f32[1,32]{1,0:T(1,128)}) custom-call(bf16[32,256]{1,0:T(8,128)(2,1)S(1)} %get-tuple-element.12.refs_0_, f32[32,128,128]{2,1,0:T(8,128)S(1)} %get-tuple-element.13.refs_1_, f32[32,128]{1,0:T(8,128)S(1)} %get-tuple-element.14.refs_2_, ...), custom_call_target="tpu_custom_call" | custom-call | tf_op jit(solution)/shard_map/write_out/pallas_call | solution.py:530

commit v8 on v7

--- a/solution.py
+++ b/solution.py
@@ -22,7 +22,7 @@
 DIRECT_IN = (0,)
 DIRECT_OUT = (4,)
 ORDER = (
-    "d", "f2", "f6", "r0", "r1", "f3", "f5", "r2", "r3", "f4", "w", "m17", "m26", "m35", "m4", "m0", "z", "s2", "s6", "s3", "s5", "s0",
+    "d", "f2", "f6", "f3", "f5", "r0", "r1", "r2", "r3", "f4", "w", "m17", "m26", "m35", "m4", "m0", "z", "s2", "s6", "s3", "s5", "s0",
 )
 ZPOS = tuple(ZORD.index(o) for o in range(ZN))
 HOME = ZPOS[0]

time: 44.6 us -> 44.6 us (level)
  no operation moved by 1% of the time
where the time goes in v8:
time: 44.6 us; the launch traced here: 44.5 us
  Pallas kernels  43.9 us (98%)
  between operations  0.65 us (1%)
    pallas_call x1, Pallas kernels, per_device(): pl.pallas_call(kernel, out_shape=outs, in_specs=[hbm] * 17, out_specs=(vm...  42.5 us
    pallas_call x1, Pallas kernels, per_device(): pl.pallas_call(write_out, out_shape=outs, in_specs=[anywhere] * 4, out_sp...  1.36 us

profile of v8, /device:TPU:1, one launch (start us, length us, event | category | flops | bytes accessed | tf_op | source)
XLA Modules:
  0.0 44.5 jit_solution(14525688098867248811)
XLA Ops:
  0.6 42.5 %layer.1 = (bf16[32,256]{1,0:T(8,128)(2,1)S(1)}, f32[32,128,128]{2,1,0:T(8,128)S(1)}, f32[32,128]{1,0:T(8,128)S(1)}, f32[1,32]{1,0:T(1,128)S(1)}) custom-call(bf16[32,256]{1,0:T(8,128)(2,1)} %tok_h.1, f32[32,128,128]{2,1,0:T(8,128)} %bitcast.16, f32[32,128]{1,0:T(8,128)} %bitcast.19, f32[1,32]{1,0:T(1,128)} %bitcast.22, f32[1,2048]{1,0:T(1,128)} %bitcast.20, ...), custom_call_target="tpu_custom_call" | custom-call | tf_op jit(solution)/shard_map/layer/pallas_call | solution.py:454
  43.1 1.4 %write_out.1 = (bf16[32,256]{1,0:T(8,128)(2,1)}, f32[32,128,128]{2,1,0:T(8,128)}, f32[32,128]{1,0:T(8,128)}, f32[1,32]{1,0:T(1,128)}) custom-call(bf16[32,256]{1,0:T(8,128)(2,1)S(1)} %get-tuple-element.12.refs_0_, f32[32,128,128]{2,1,0:T(8,128)S(1)} %get-tuple-element.13.refs_1_, f32[32,128]{1,0:T(8,128)S(1)} %get-tuple-element.14.refs_2_, ...), custom_call_target="tpu_custom_call" | custom-call | tf_op jit(solution)/shard_map/write_out/pallas_call | solution.py:530
